TPU v7x, 256 devices: a 8x8x2 block of a 8x8x16 slice. The times are simulated.
256 devices in a mesh: grp: 2 (over z), sp: 64 (over y, x), tp: 2 (over core).
Axes of the slice: x: 8, y: 8, z: 2, core: 2. Of those that a mesh axis runs over, the one named last changes fastest.
The devices are a block of a 8x8x16 slice.
Arguments:
- resid: bfloat16 [16384, 2048], P(('grp', 'sp')), parts along dimension 0, may hold values from -6 to 6
- queries_first: bfloat16 [16384, 2048], P(('grp', 'sp'), 'tp'), parts along dimension 0, may hold values from -150 to 150
- keys_first: bfloat16 [16384, 2048], P(('grp', 'sp'), 'tp'), parts along dimension 0, may hold values from -6 to 6
- values_first: bfloat16 [16384, 2048], P(('grp', 'sp'), 'tp'), parts along dimension 0, may hold values from -6 to 6
- rel_first: float32 [16, 257], P('tp'), may hold values from -4 to 4
- post_first: float32 [2048], replicated, may hold values from 0.1 to 1.9
- out_first: bfloat16 [2048, 2048], P('tp', 'sp'), may hold values from -0.125 to 0.125
- pre_second: float32 [2048], replicated, may hold values from 0.1 to 1.9
- query_weight: bfloat16 [2048, 2048], P('sp', 'tp'), may hold values from -0.125 to 0.125
- key_weight: bfloat16 [2048, 2048], P('sp', 'tp'), may hold values from -0.125 to 0.125
- value_weight: bfloat16 [2048, 2048], P('sp', 'tp'), may hold values from -0.125 to 0.125
- rel_second: float32 [16, 257], P('tp'), may hold values from -4 to 4
- post_second: float32 [2048], replicated, may hold values from 0.1 to 1.9
- out_second: bfloat16 [2048, 2048], P('tp', 'sp'), may hold values from -0.125 to 0.125
Outputs:
- hidden_two: bfloat16 [16384, 2048], P(('grp', 'sp')), parts along dimension 0
There are 2 independent parts, one for each index of `grp`. A program takes and returns all parts, laid end to end along the dimension named above; an argument that names none is the same for every part. Nothing has to cross between parts.
All inputs are finite; a program needn't handle non-finite values.
Results may differ from a plain program's by a relative error of at most 0.017.
Values may be sent and summed in bfloat16 or wider, within the bound.
A program may use at most 128 MiB of HBM per device.

v0:
```python
import jax
import jax.numpy as jnp
from jax import lax
from jax.sharding import PartitionSpec as P

SEG = 64
LEFT = 8
REACH = 512
REL_CLIP = 128


EPS = 1e-06
NEG_FILL = -1e30


def sent_to_all(shard, axis):
    copies = jnp.broadcast_to(shard, (lax.axis_size(axis), *shard.shape))
    return lax.all_to_all(copies, axis, split_axis=0, concat_axis=0, tiled=True)


def over_copies(shard, axis):
    return sent_to_all(shard, axis).astype(jnp.float32).sum(axis=0)


def from_behind(value, axis, steps):
    count = lax.axis_size(axis)
    initial, last = (max(0, -steps), min(count, count - steps))
    return lax.ppermute(value, axis, [(source, source + steps) for source in range(initial, last)])


def in_one_piece(arrays, axis, dim, along):
    both = jnp.concatenate(arrays, axis=along)
    whole, at, finished = (lax.all_gather(both, axis, axis=dim, tiled=True), 0, [])
    for a in arrays:
        finished.append(lax.slice_in_dim(whole, at, at + a.shape[along], axis=along))
        at += a.shape[along]
    return tuple(finished)


def band_bias(bias_table):
    heads_here = bias_table.shape[0]
    band = (LEFT + 1) * SEG
    length = SEG + band
    index = jnp.arange(length, dtype=jnp.int32)
    distance = jnp.where(index < band, LEFT * SEG - index, LEFT * SEG + length - index)
    slot = jnp.clip(distance, -REL_CLIP, REL_CLIP) + REL_CLIP
    onehot = (slot[:, None] == jnp.arange(2 * REL_CLIP + 1, dtype=jnp.int32)[None, :]).astype(
        jnp.float32
    )
    diagonal_values = jnp.dot(bias_table, onehot.T, precision=lax.Precision.HIGHEST)
    spread = jnp.broadcast_to(diagonal_values[:, None, :], (heads_here, SEG, length)).reshape(
        heads_here, SEG * length
    )
    return spread[:, : SEG * (length - 1)].reshape(heads_here, SEG, length - 1)[:, :, :band]


def attend_band(queries, key_rows, value_rows, bias, key_live):
    rows, width = queries.shape
    heads_here = bias.shape[0]
    head_size = width // heads_here
    blocks = rows // SEG
    query_seg = queries.reshape(blocks, SEG, heads_here, head_size)
    key_seg = key_rows.reshape(blocks + LEFT, SEG, heads_here, head_size)
    value_seg = value_rows.reshape(blocks + LEFT, SEG, heads_here, head_size)
    live_seg = key_live.reshape(blocks + LEFT, SEG)
    key_band = jnp.concatenate(
        [key_seg[earlier : earlier + blocks] for earlier in range(LEFT + 1)], axis=1
    )
    value_band = jnp.concatenate(
        [value_seg[earlier : earlier + blocks] for earlier in range(LEFT + 1)], axis=1
    )
    live_band = jnp.concatenate(
        [live_seg[earlier : earlier + blocks] for earlier in range(LEFT + 1)], axis=1
    )
    scores = jnp.einsum("nqhd,nkhd->nhqk", query_seg, key_band, preferred_element_type=jnp.float32)
    scores = scores * head_size ** (-0.5) + bias[None]
    scores = jnp.where(live_band[:, None, None, :], scores, NEG_FILL)
    largest = jnp.max(scores, axis=-1, keepdims=True)
    weights = jnp.exp(scores - largest)
    weights = (weights / jnp.sum(weights, axis=-1, keepdims=True)).astype(jnp.bfloat16)
    mixed = jnp.einsum("nhqk,nkhd->nqhd", weights, value_band, preferred_element_type=jnp.float32)
    return mixed.astype(jnp.bfloat16).reshape(rows, width)


def extend_rows(pieces, member, own_rows):
    joined = jnp.concatenate([piece[member] for piece in pieces] + [own_rows], axis=0)
    return joined


def normed(hidden, gain):
    values = hidden.astype(jnp.float32)
    scale = lax.rsqrt(jnp.mean(values * values, axis=-1, keepdims=True) + EPS)
    return (values * scale * gain).astype(jnp.bfloat16)


def residual_add(branch, residual, gain):
    values = branch.astype(jnp.float32)
    scale = lax.rsqrt(jnp.mean(values * values, axis=-1, keepdims=True) + EPS)
    return (residual.astype(jnp.float32) + values * scale * gain).astype(jnp.bfloat16)


def combine(mixed, weight, residual, gain):
    partial_rows = jnp.dot(
        mixed, lax.all_gather(weight, "sp", axis=1, tiled=True), preferred_element_type=jnp.float32
    )
    branch = (
        over_copies(partial_rows.astype(jnp.bfloat16), "tp")
        .astype(jnp.float32)
        .astype(jnp.bfloat16)
    )
    return residual_add(branch, residual, gain)


def shards(
    resid,
    queries_first,
    keys_first,
    values_first,
    rel_first,
    post_first,
    out_first,
    pre_second,
    query_weight,
    key_weight,
    value_weight,
    rel_second,
    post_second,
    out_second,
):
    tok_rows = resid.shape[0]
    depth = (REACH + tok_rows - 1) // tok_rows
    anchor = lax.axis_index("sp") * tok_rows
    key_live = anchor - REACH + jnp.arange(tok_rows + REACH, dtype=jnp.int32) >= 0
    earlier_first = [
        from_behind((keys_first, values_first), "sp", distance) for distance in range(depth, 0, -1)
    ]
    key_ext = extend_rows(earlier_first, 0, keys_first)
    value_ext = extend_rows(earlier_first, 1, values_first)
    first = attend_band(queries_first, key_ext, value_ext, band_bias(rel_first), key_live)
    hidden_one = combine(first, out_first, resid, post_first)
    inputs_two = normed(hidden_one, pre_second)
    pieces = in_one_piece((query_weight, key_weight, value_weight), "sp", 0, 1)
    query_sum = jnp.dot(inputs_two, pieces[0], preferred_element_type=jnp.float32)
    key_sum = jnp.dot(inputs_two, pieces[1], preferred_element_type=jnp.float32)
    value_sum = jnp.dot(inputs_two, pieces[2], preferred_element_type=jnp.float32)
    queries_two = query_sum.astype(jnp.bfloat16)
    keys_two = key_sum.astype(jnp.bfloat16)
    values_two = value_sum.astype(jnp.bfloat16)
    earlier_second = [
        from_behind((keys_two, values_two), "sp", distance) for distance in range(depth, 0, -1)
    ]
    key_ext_two = extend_rows(earlier_second, 0, keys_two)
    value_ext_two = extend_rows(earlier_second, 1, values_two)
    second = attend_band(queries_two, key_ext_two, value_ext_two, band_bias(rel_second), key_live)
    hidden_two = combine(second, out_second, hidden_one, post_second)
    return hidden_two


def solution(mesh):
    in_specs = (
        P(("grp", "sp"), None),
        P(("grp", "sp"), "tp"),
        P(("grp", "sp"), "tp"),
        P(("grp", "sp"), "tp"),
        P("tp", None),
        P(),
        P("tp", "sp"),
        P(),
        P("sp", "tp"),
        P("sp", "tp"),
        P("sp", "tp"),
        P("tp", None),
        P(),
        P("tp", "sp"),
    )
    out_specs = P(("grp", "sp"), None)
    return jax.shard_map(shards, mesh=mesh, in_specs=in_specs, out_specs=out_specs, check_vma=False)
```

profile of v0, /device:TPU:513, one launch (start us, length us, event | category | flops | bytes accessed | tf_op | source)
XLA Modules:
  0.0 416.6 jit_solution(2990018467592462493)
XLA Ops:
  9.1 8.5 %collective-permute-start.4 = (bf16[128,1024]{1,0:T(8,128)(2,1)}, bf16[128,1024]{1,0:T(8,128)(2,1)S(1)}, u32[]{:S(2)}, u32[]{:S(2)}) collective-permute-start(bf16[128,1024]{1,0:T(8,128)(2,1)} %param.16), channel_id=1, source_target_pairs={{0,8},{2,10},{4,12},{6,14},{8,16},{10,18},{12,20},{14,22},{16,24},... | collective-permute-start | bytes 786440 | tf_op jit(solution)/shard_map/ppermute | solution.py:28
  20.4 4.4 %collective-permute-start.6 = (bf16[128,1024]{1,0:T(8,128)(2,1)}, bf16[128,1024]{1,0:T(8,128)(2,1)S(1)}, u32[]{:S(2)}, u32[]{:S(2)}) collective-permute-start(bf16[128,1024]{1,0:T(8,128)(2,1)} %param.16), channel_id=1, source_target_pairs={{0,4},{2,6},{4,8},{6,10},{8,12},{10,14},{12,16},{14,18},{16,20},{1... | collective-permute-start | bytes 786440 | tf_op jit(solution)/shard_map/ppermute | solution.py:28
  28.0 5.9 %collective-permute-start = (bf16[128,1024]{1,0:T(8,128)(2,1)}, bf16[128,1024]{1,0:T(8,128)(2,1)S(1)}, u32[]{:S(2)}, u32[]{:S(2)}) collective-permute-start(bf16[128,1024]{1,0:T(8,128)(2,1)} %param.17), channel_id=1, source_target_pairs={{0,8},{2,10},{4,12},{6,14},{8,16},{10,18},{12,20},{14,22},{16,24},... | collective-permute-start | bytes 786440 | tf_op jit(solution)/shard_map/ppermute | solution.py:28
  43.6 4.5 %collective-permute-start.1 = (bf16[128,1024]{1,0:T(8,128)(2,1)S(1)}, bf16[128,1024]{1,0:T(8,128)(2,1)S(1)}, u32[]{:S(2)}, u32[]{:S(2)}) collective-permute-start(bf16[128,1024]{1,0:T(8,128)(2,1)S(1)} %copy-done.3), channel_id=1, source_target_pairs={{0,6},{2,8},{4,10},{6,12},{8,14},{10,16},{12,18},{14,20},{16,22},{... | collective-permute-start | bytes 786440 | tf_op jit(solution)/shard_map/ppermute | solution.py:28
  48.2 4.3 %collective-permute-start.2 = (bf16[128,1024]{1,0:T(8,128)(2,1)S(1)}, bf16[128,1024]{1,0:T(8,128)(2,1)S(1)}, u32[]{:S(2)}, u32[]{:S(2)}) collective-permute-start(bf16[128,1024]{1,0:T(8,128)(2,1)S(1)} %copy-done.3), channel_id=1, source_target_pairs={{0,4},{2,6},{4,8},{6,10},{8,12},{10,14},{12,16},{14,18},{16,20},{1... | collective-permute-start | bytes 786440 | tf_op jit(solution)/shard_map/ppermute | solution.py:28
  52.5 8.0 %collective-permute-start.3 = (bf16[128,1024]{1,0:T(8,128)(2,1)S(1)}, bf16[128,1024]{1,0:T(8,128)(2,1)S(1)}, u32[]{:S(2)}, u32[]{:S(2)}) collective-permute-start(bf16[128,1024]{1,0:T(8,128)(2,1)S(1)} %copy-done.3), channel_id=1, source_target_pairs={{0,2},{2,4},{4,6},{6,8},{8,10},{10,12},{12,14},{14,16},{16,18},{18... | collective-permute-start | bytes 786440 | tf_op jit(solution)/shard_map/ppermute | solution.py:28
  64.4 6.0 %collective-permute-done.1 = bf16[128,1024]{1,0:T(8,128)(2,1)S(1)} collective-permute-done((bf16[128,1024]{1,0:T(8,128)(2,1)S(1)}, bf16[128,1024]{1,0:T(8,128)(2,1)S(1)}, u32[]{:S(2)}, u32[]{:S(2)}) %collective-permute-start.1) | collective-permute-done | bytes 262176 | tf_op jit(solution)/shard_map/ppermute | solution.py:28
  70.4 18.9 %collective-permute-done.2 = bf16[128,1024]{1,0:T(8,128)(2,1)S(1)} collective-permute-done((bf16[128,1024]{1,0:T(8,128)(2,1)S(1)}, bf16[128,1024]{1,0:T(8,128)(2,1)S(1)}, u32[]{:S(2)}, u32[]{:S(2)}) %collective-permute-start.2) | collective-permute-done | bytes 262176 | tf_op jit(solution)/shard_map/ppermute | solution.py:28
  89.3 9.4 %collective-permute-done.3 = bf16[128,1024]{1,0:T(8,128)(2,1)S(1)} collective-permute-done((bf16[128,1024]{1,0:T(8,128)(2,1)S(1)}, bf16[128,1024]{1,0:T(8,128)(2,1)S(1)}, u32[]{:S(2)}, u32[]{:S(2)}) %collective-permute-start.3) | collective-permute-done | bytes 262176 | tf_op jit(solution)/shard_map/ppermute | solution.py:28
  119.5 5.0 %fusion.36 = bf16[2,64,8,128]{3,1,2,0:T(8,128)(2,1)S(1)} fusion(bf16[2,576,8,128]{3,1,2,0:T(8,128)(2,1)} %copy_dynamic-update-slice_fusion.27, f32[2,8,64]{2,1,0:T(8,128)S(1)} %fusion.108, f32[2,8,576,64]{2,3,1,0:T(8,128)} %fusion.72, f32[8,64,576]{2,1,0:T(8,128)} %bitcast.183, pred[2,576]{1,0:T(4,128)(4,1)S(1)} %concatenate.76), kind=kOutput, calls=%fused_computation.42 | convolution fusion | flops 154666560 | bytes 6165632 | tf_op jit(solution)/shard_map/nhqk,nkhd->nqhd/dot_general | solution.py:81
  124.7 18.5 %all-gather.4.cloned.1.call-done = bf16[1024,2048]{0,1:T(8,128)(2,1)} async-done(((bf16[1024,32]{0,1:T(8,128)(2,1)}), bf16[1024,2048]{0,1:T(8,128)(2,1)}) %all-gather.4.cloned.1.call-update) | async-done | bytes 4194320 | tf_op jit(solution)/shard_map/all_gather | solution.py:104
  147.0 8.0 %all_to_all.10 = bf16[2,128,2048]{2,1,0:T(8,128)(2,1)S(1)} all-to-all(bf16[2,128,2048]{2,1,0:T(8,128)(2,1)S(1)} %broadcast_in_dim.27), channel_id=1, replica_groups=mesh['grp'=2,'sp'=64,'tp'=2] {'tp'}, dimensions={0} | all-to-all | bytes 2097152 | tf_op jit(solution)/shard_map/all_to_all | solution.py:18
  155.9 113.4 %all-gather.6.cloned.1.call-done = bf16[2048,3072]{1,0:T(8,128)(2,1)} async-done(((bf16[32,3072]{1,0:T(8,128)(2,1)}), bf16[2048,3072]{1,0:T(8,128)(2,1)}) %all-gather.6.cloned.1.call-update) | async-done | bytes 12582928 | tf_op jit(solution)/shard_map/all_gather | solution.py:33
  272.3 7.1 %collective-permute-start.12 = (bf16[128,1024]{1,0:T(8,128)(2,1)S(1)}, bf16[128,1024]{1,0:T(8,128)(2,1)S(1)}, u32[]{:S(2)}, u32[]{:S(2)}) collective-permute-start(bf16[128,1024]{1,0:T(8,128)(2,1)S(1)} %fusion.27), channel_id=1, source_target_pairs={{0,8},{2,10},{4,12},{6,14},{8,16},{10,18},{12,20},{14,22},{16,24},... | collective-permute-start | bytes 786440 | tf_op jit(solution)/shard_map/ppermute | solution.py:28
  290.2 5.3 %collective-permute-start.10 = (bf16[128,1024]{1,0:T(8,128)(2,1)S(1)}, bf16[128,1024]{1,0:T(8,128)(2,1)S(1)}, u32[]{:S(2)}, u32[]{:S(2)}) collective-permute-start(bf16[128,1024]{1,0:T(8,128)(2,1)S(1)} %fusion.30), channel_id=1, source_target_pairs={{0,4},{2,6},{4,8},{6,10},{8,12},{10,14},{12,16},{14,18},{16,20},{1... | collective-permute-start | bytes 786440 | tf_op jit(solution)/shard_map/ppermute | solution.py:28
  297.7 8.2 %collective-permute-done.13 = bf16[128,1024]{1,0:T(8,128)(2,1)S(1)} collective-permute-done((bf16[128,1024]{1,0:T(8,128)(2,1)S(1)}, bf16[128,1024]{1,0:T(8,128)(2,1)S(1)}, u32[]{:S(2)}, u32[]{:S(2)}) %collective-permute-start.13) | collective-permute-done | bytes 262176 | tf_op jit(solution)/shard_map/ppermute | solution.py:28
  305.8 11.5 %collective-permute-start.8 = (bf16[128,1024]{1,0:T(8,128)(2,1)S(1)}, bf16[128,1024]{1,0:T(8,128)(2,1)S(1)}, u32[]{:S(2)}, u32[]{:S(2)}) collective-permute-start(bf16[128,1024]{1,0:T(8,128)(2,1)S(1)} %fusion.30), channel_id=1, source_target_pairs={{0,8},{2,10},{4,12},{6,14},{8,16},{10,18},{12,20},{14,22},{16,24},... | collective-permute-start | bytes 786440 | tf_op jit(solution)/shard_map/ppermute | solution.py:28
  317.4 9.4 %collective-permute-start.9 = (bf16[128,1024]{1,0:T(8,128)(2,1)S(1)}, bf16[128,1024]{1,0:T(8,128)(2,1)S(1)}, u32[]{:S(2)}, u32[]{:S(2)}) collective-permute-start(bf16[128,1024]{1,0:T(8,128)(2,1)S(1)} %fusion.30), channel_id=1, source_target_pairs={{0,6},{2,8},{4,10},{6,12},{8,14},{10,16},{12,18},{14,20},{16,22},{... | collective-permute-start | bytes 786440 | tf_op jit(solution)/shard_map/ppermute | solution.py:28
  331.4 15.9 %collective-permute-done.11 = bf16[128,1024]{1,0:T(8,128)(2,1)S(1)} collective-permute-done((bf16[128,1024]{1,0:T(8,128)(2,1)S(1)}, bf16[128,1024]{1,0:T(8,128)(2,1)S(1)}, u32[]{:S(2)}, u32[]{:S(2)}) %collective-permute-start.11) | collective-permute-done | bytes 262176 | tf_op jit(solution)/shard_map/ppermute | solution.py:28
  347.3 15.2 %collective-permute-done.8 = bf16[128,1024]{1,0:T(8,128)(2,1)S(1)} collective-permute-done((bf16[128,1024]{1,0:T(8,128)(2,1)S(1)}, bf16[128,1024]{1,0:T(8,128)(2,1)S(1)}, u32[]{:S(2)}, u32[]{:S(2)}) %collective-permute-start.8) | collective-permute-done | bytes 262176 | tf_op jit(solution)/shard_map/ppermute | solution.py:28
  362.6 20.5 %collective-permute-done.9 = bf16[128,1024]{1,0:T(8,128)(2,1)S(1)} collective-permute-done((bf16[128,1024]{1,0:T(8,128)(2,1)S(1)}, bf16[128,1024]{1,0:T(8,128)(2,1)S(1)}, u32[]{:S(2)}, u32[]{:S(2)}) %collective-permute-start.9) | collective-permute-done | bytes 262176 | tf_op jit(solution)/shard_map/ppermute | solution.py:28
  391.5 4.9 %fusion.37 = bf16[2,64,8,128]{3,1,2,0:T(8,128)(2,1)S(1)} fusion(bf16[2,576,8,128]{3,1,2,0:T(8,128)(2,1)} %copy-done.9, f32[2,8,64]{2,1,0:T(8,128)S(1)} %fusion.111, f32[2,8,64,576]{3,2,1,0:T(8,128)} %fusion.70, f32[8,64,576]{2,1,0:T(8,128)} %bitcast.181, pred[2,576]{1,0:T(4,128)(4,1)S(1)} %concatenate.76), kind=kOutput, calls=%fused_computation.43 | convolution fusion | flops 154666560 | bytes 6165632 | tf_op jit(solution)/shard_map/nhqk,nkhd->nqhd/dot_general | solution.py:81
  396.6 3.7 convolution_convert_fusion
  400.4 8.0 %all_to_all.11 = bf16[2,128,2048]{2,1,0:T(8,128)(2,1)S(1)} all-to-all(bf16[2,128,2048]{2,1,0:T(8,128)(2,1)S(1)} %broadcast_in_dim.29), channel_id=1, replica_groups=mesh['grp'=2,'sp'=64,'tp'=2] {'tp'}, dimensions={0} | all-to-all | bytes 2097152 | tf_op jit(solution)/shard_map/all_to_all | solution.py:18
  (158 shorter events, 78.2 us)
Async XLA Ops:
  6.5 27.5 %copy-start = (f32[8,257]{1,0:T(8,128)S(1)}, f32[8,257]{1,0:T(8,128)}, u32[]{:S(2)}) copy-start(f32[8,257]{1,0:T(8,128)} %param.18) | copy-start | bytes 24676
  6.6 136.6 %all-gather.4.cloned.1.call-start = ((), (), s32[]{:S(2)}) async-start(), calls=%async_computation.2 | async-start | bytes 4259840 | tf_op jit(solution)/shard_map/all_gather | solution.py:104
  7.3 262.0 %all-gather.6.cloned.1.call-start = ((), (), s32[]{:S(2)}) async-start(), calls=%async_computation.3 | async-start | bytes 12779520 | tf_op jit(solution)/shard_map/all_gather | solution.py:33
  9.0 387.5 %all-gather.8.cloned.1.call-start = ((), (), s32[]{:S(2)}) async-start(), calls=%async_computation.4 | async-start | bytes 4259840 | tf_op jit(solution)/shard_map/all_gather | solution.py:104
  9.1 34.5 %collective-permute-start.4 = (bf16[128,1024]{1,0:T(8,128)(2,1)}, bf16[128,1024]{1,0:T(8,128)(2,1)S(1)}, u32[]{:S(2)}, u32[]{:S(2)}) collective-permute-start(bf16[128,1024]{1,0:T(8,128)(2,1)} %param.16), channel_id=1, source_target_pairs={{0,8},{2,10},{4,12},{6,14},{8,16},{10,18},{12,20},{14,22},{16,24},... | collective-permute-start | bytes 786440 | tf_op jit(solution)/shard_map/ppermute | solution.py:28
  17.6 30.5 %collective-permute-start.5 = (bf16[128,1024]{1,0:T(8,128)(2,1)}, bf16[128,1024]{1,0:T(8,128)(2,1)S(1)}, u32[]{:S(2)}, u32[]{:S(2)}) collective-permute-start(bf16[128,1024]{1,0:T(8,128)(2,1)} %param.16), channel_id=1, source_target_pairs={{0,6},{2,8},{4,10},{6,12},{8,14},{10,16},{12,18},{14,20},{16,22},{... | collective-permute-start | bytes 786440 | tf_op jit(solution)/shard_map/ppermute | solution.py:28
  20.4 32.2 %collective-permute-start.6 = (bf16[128,1024]{1,0:T(8,128)(2,1)}, bf16[128,1024]{1,0:T(8,128)(2,1)S(1)}, u32[]{:S(2)}, u32[]{:S(2)}) collective-permute-start(bf16[128,1024]{1,0:T(8,128)(2,1)} %param.16), channel_id=1, source_target_pairs={{0,4},{2,6},{4,8},{6,10},{8,12},{10,14},{12,16},{14,18},{16,20},{1... | collective-permute-start | bytes 786440 | tf_op jit(solution)/shard_map/ppermute | solution.py:28
  24.7 35.8 %collective-permute-start.7 = (bf16[128,1024]{1,0:T(8,128)(2,1)}, bf16[128,1024]{1,0:T(8,128)(2,1)S(1)}, u32[]{:S(2)}, u32[]{:S(2)}) collective-permute-start(bf16[128,1024]{1,0:T(8,128)(2,1)} %param.16), channel_id=1, source_target_pairs={{0,2},{2,4},{4,6},{6,8},{8,10},{10,12},{12,14},{14,16},{16,18},{18... | collective-permute-start | bytes 786440 | tf_op jit(solution)/shard_map/ppermute | solution.py:28
  28.0 36.3 %collective-permute-start = (bf16[128,1024]{1,0:T(8,128)(2,1)}, bf16[128,1024]{1,0:T(8,128)(2,1)S(1)}, u32[]{:S(2)}, u32[]{:S(2)}) collective-permute-start(bf16[128,1024]{1,0:T(8,128)(2,1)} %param.17), channel_id=1, source_target_pairs={{0,8},{2,10},{4,12},{6,14},{8,16},{10,18},{12,20},{14,22},{16,24},... | collective-permute-start | bytes 786440 | tf_op jit(solution)/shard_map/ppermute | solution.py:28
  40.3 20.3 %copy-start.2 = (bf16[128,1024]{1,0:T(8,128)(2,1)S(1)}, bf16[128,1024]{1,0:T(8,128)(2,1)}, u32[]{:S(2)}) copy-start(bf16[128,1024]{1,0:T(8,128)(2,1)} %param.16) | copy-start | bytes 786436
  43.6 26.8 %collective-permute-start.1 = (bf16[128,1024]{1,0:T(8,128)(2,1)S(1)}, bf16[128,1024]{1,0:T(8,128)(2,1)S(1)}, u32[]{:S(2)}, u32[]{:S(2)}) collective-permute-start(bf16[128,1024]{1,0:T(8,128)(2,1)S(1)} %copy-done.3), channel_id=1, source_target_pairs={{0,6},{2,8},{4,10},{6,12},{8,14},{10,16},{12,18},{14,20},{16,22},{... | collective-permute-start | bytes 786440 | tf_op jit(solution)/shard_map/ppermute | solution.py:28
  48.2 41.1 %collective-permute-start.2 = (bf16[128,1024]{1,0:T(8,128)(2,1)S(1)}, bf16[128,1024]{1,0:T(8,128)(2,1)S(1)}, u32[]{:S(2)}, u32[]{:S(2)}) collective-permute-start(bf16[128,1024]{1,0:T(8,128)(2,1)S(1)} %copy-done.3), channel_id=1, source_target_pairs={{0,4},{2,6},{4,8},{6,10},{8,12},{10,14},{12,16},{14,18},{16,20},{1... | collective-permute-start | bytes 786440 | tf_op jit(solution)/shard_map/ppermute | solution.py:28
  52.5 46.1 %collective-permute-start.3 = (bf16[128,1024]{1,0:T(8,128)(2,1)S(1)}, bf16[128,1024]{1,0:T(8,128)(2,1)S(1)}, u32[]{:S(2)}, u32[]{:S(2)}) collective-permute-start(bf16[128,1024]{1,0:T(8,128)(2,1)S(1)} %copy-done.3), channel_id=1, source_target_pairs={{0,2},{2,4},{4,6},{6,8},{8,10},{10,12},{12,14},{14,16},{16,18},{18... | collective-permute-start | bytes 786440 | tf_op jit(solution)/shard_map/ppermute | solution.py:28
  109.5 9.2 %copy-start.4 = (bf16[16,8,8,128]{3,2,1,0:T(8,128)(2,1)S(1)}, bf16[16,8,8,128]{3,2,1,0:T(8,128)(2,1)}, u32[]{:S(2)}) copy-start(bf16[16,8,8,128]{3,2,1,0:T(8,128)(2,1)} %copy.133) | copy-start | bytes 786436
  155.0 114.3 %copy-start.12 = (f32[2048]{0:T(1024)S(1)}, f32[2048]{0:T(1024)}, u32[]{:S(2)}) copy-start(f32[2048]{0:T(1024)} %param.21) | copy-start | bytes 24580
  272.3 23.1 %collective-permute-start.12 = (bf16[128,1024]{1,0:T(8,128)(2,1)S(1)}, bf16[128,1024]{1,0:T(8,128)(2,1)S(1)}, u32[]{:S(2)}, u32[]{:S(2)}) collective-permute-start(bf16[128,1024]{1,0:T(8,128)(2,1)S(1)} %fusion.27), channel_id=1, source_target_pairs={{0,8},{2,10},{4,12},{6,14},{8,16},{10,18},{12,20},{14,22},{16,24},... | collective-permute-start | bytes 786440 | tf_op jit(solution)/shard_map/ppermute | solution.py:28
  279.4 26.4 %collective-permute-start.13 = (bf16[128,1024]{1,0:T(8,128)(2,1)S(1)}, bf16[128,1024]{1,0:T(8,128)(2,1)S(1)}, u32[]{:S(2)}, u32[]{:S(2)}) collective-permute-start(bf16[128,1024]{1,0:T(8,128)(2,1)S(1)} %fusion.27), channel_id=1, source_target_pairs={{0,6},{2,8},{4,10},{6,12},{8,14},{10,16},{12,18},{14,20},{16,22},{... | collective-permute-start | bytes 786440 | tf_op jit(solution)/shard_map/ppermute | solution.py:28
  281.7 35.7 %collective-permute-start.14 = (bf16[128,1024]{1,0:T(8,128)(2,1)S(1)}, bf16[128,1024]{1,0:T(8,128)(2,1)S(1)}, u32[]{:S(2)}, u32[]{:S(2)}) collective-permute-start(bf16[128,1024]{1,0:T(8,128)(2,1)S(1)} %fusion.27), channel_id=1, source_target_pairs={{0,4},{2,6},{4,8},{6,10},{8,12},{10,14},{12,16},{14,18},{16,20},{1... | collective-permute-start | bytes 786440 | tf_op jit(solution)/shard_map/ppermute | solution.py:28
  284.0 45.9 %collective-permute-start.15 = (bf16[128,1024]{1,0:T(8,128)(2,1)S(1)}, bf16[128,1024]{1,0:T(8,128)(2,1)S(1)}, u32[]{:S(2)}, u32[]{:S(2)}) collective-permute-start(bf16[128,1024]{1,0:T(8,128)(2,1)S(1)} %fusion.27), channel_id=1, source_target_pairs={{0,2},{2,4},{4,6},{6,8},{8,10},{10,12},{12,14},{14,16},{16,18},{18... | collective-permute-start | bytes 786440 | tf_op jit(solution)/shard_map/ppermute | solution.py:28
  290.2 41.3 %collective-permute-start.10 = (bf16[128,1024]{1,0:T(8,128)(2,1)S(1)}, bf16[128,1024]{1,0:T(8,128)(2,1)S(1)}, u32[]{:S(2)}, u32[]{:S(2)}) collective-permute-start(bf16[128,1024]{1,0:T(8,128)(2,1)S(1)} %fusion.30), channel_id=1, source_target_pairs={{0,4},{2,6},{4,8},{6,10},{8,12},{10,14},{12,16},{14,18},{16,20},{1... | collective-permute-start | bytes 786440 | tf_op jit(solution)/shard_map/ppermute | solution.py:28
  295.4 51.9 %collective-permute-start.11 = (bf16[128,1024]{1,0:T(8,128)(2,1)S(1)}, bf16[128,1024]{1,0:T(8,128)(2,1)S(1)}, u32[]{:S(2)}, u32[]{:S(2)}) collective-permute-start(bf16[128,1024]{1,0:T(8,128)(2,1)S(1)} %fusion.30), channel_id=1, source_target_pairs={{0,2},{2,4},{4,6},{6,8},{8,10},{10,12},{12,14},{14,16},{16,18},{18... | collective-permute-start | bytes 786440 | tf_op jit(solution)/shard_map/ppermute | solution.py:28
  305.8 56.7 %collective-permute-start.8 = (bf16[128,1024]{1,0:T(8,128)(2,1)S(1)}, bf16[128,1024]{1,0:T(8,128)(2,1)S(1)}, u32[]{:S(2)}, u32[]{:S(2)}) collective-permute-start(bf16[128,1024]{1,0:T(8,128)(2,1)S(1)} %fusion.30), channel_id=1, source_target_pairs={{0,8},{2,10},{4,12},{6,14},{8,16},{10,18},{12,20},{14,22},{16,24},... | collective-permute-start | bytes 786440 | tf_op jit(solution)/shard_map/ppermute | solution.py:28
  317.4 65.7 %collective-permute-start.9 = (bf16[128,1024]{1,0:T(8,128)(2,1)S(1)}, bf16[128,1024]{1,0:T(8,128)(2,1)S(1)}, u32[]{:S(2)}, u32[]{:S(2)}) collective-permute-start(bf16[128,1024]{1,0:T(8,128)(2,1)S(1)} %fusion.30), channel_id=1, source_target_pairs={{0,6},{2,8},{4,10},{6,12},{8,14},{10,16},{12,18},{14,20},{16,22},{... | collective-permute-start | bytes 786440 | tf_op jit(solution)/shard_map/ppermute | solution.py:28
  400.4 9.6 %copy-start.1 = (f32[8,257]{1,0:T(8,128)S(1)}, f32[8,257]{1,0:T(8,128)}, u32[]{:S(2)}) copy-start(f32[8,257]{1,0:T(8,128)} %param.18) | copy-start | bytes 24676
  (8 other events, 38.7 us)
Sparse Core Ops, SparseCore 0:
  9.9 133.2 all-gather.3
  145.6 123.6 all-gather.5
  271.8 122.7 all-gather.7
where the time goes:
time: 418 us; the launch traced here: 417 us
  waiting for transfers between devices  231 us (55%)
  starting transfers between devices  84.9 us (20%)
  matrix products  38.3 us (9%)
  local copies, waits for them, and re-layouts  27.8 us (7%)
  blocking collectives  16 us (4%)
  between operations  14.1 us (3%)
  other arithmetic  4.4 us (1%)
    all_gather x1, waiting for transfers between devices, in_one_piece(): lax.all_gather(both, axis, axis=dim, tiled=True)  113 us
    ppermute x16, waiting for transfers between devices, from_behind(): lax.ppermute(value, axis, [(source, source + steps) for source in range(i...  98.4 us
    ppermute x16, starting transfers between devices, from_behind(): lax.ppermute(value, axis, [(source, source + steps) for source in range(i...  84.8 us
    unnamed x96, local copies, waits for them, and re-layouts  21.1 us
    all_gather x2, waiting for transfers between devices, combine(): lax.all_gather(weight, 'sp', axis=1, tiled=True)  18.5 us
    all_to_all x2, blocking collectives, sent_to_all(): return lax.all_to_all(copies, axis, split_axis=0, concat_axis=0, tiled=True)  16 us
    dot_general x2, matrix products, attend_band(): jnp.einsum('nhqk,nkhd->nqhd', weights, value_band, preferred_element_type...  9.85 us
  transfers between devices with their start and end apart: 19, of which 11 were waited for; matrix products, arithmetic and copies ran while one was open for 15% of the time, Pallas kernels for 0%

commit v1 on v0

v1 whole, which is shorter than its diff:
```python
import functools
import math

import jax
import jax.numpy as jnp
from jax import lax
from jax.experimental import pallas as pl
from jax.experimental.pallas import tpu as pltpu
from jax.sharding import PartitionSpec as P

SEG = 64
LEFT = 8
REACH = 512
REL_CLIP = 128
EPS = 1e-06
NEG_FILL = -1e30
LOG2E = 1.4426950408889634
BF = jnp.bfloat16
F32 = jnp.float32
MESH = pl.DeviceIdType.MESH
VM = pl.BlockSpec(memory_space=pltpu.VMEM)
ANY = pl.BlockSpec(memory_space=pl.ANY)
NT = (((1,), (1,)), ((), ()))


def place(side):
    sp = lax.axis_index("sp")
    return lax.rem(sp, side), lax.div(sp, side), lax.axis_index("tp")


def remote(src, dst, send, recv, **where):
    return pltpu.make_async_remote_copy(
        src_ref=src,
        dst_ref=dst,
        send_sem=send,
        recv_sem=recv,
        device_id=dict(where),
        device_id_type=MESH,
    )


def greet(side, x, y, rows, core):
    barrier = pltpu.get_barrier_semaphore()
    count = 0
    if rows:
        for d in range(1, side):
            peer = y * side + lax.rem(x + d, side)
            pl.semaphore_signal(barrier, inc=1, device_id={"sp": peer}, device_id_type=MESH)
            count += 1
        for d in (1, side - 1):
            peer = lax.rem(y + d, side) * side + x
            pl.semaphore_signal(barrier, inc=1, device_id={"sp": peer}, device_id_type=MESH)
            count += 1
    if core:
        pl.semaphore_signal(
            barrier, inc=1, device_id={"tp": 1 - lax.axis_index("tp")}, device_id_type=MESH
        )
        count += 1
    pl.semaphore_wait(barrier, count)


def spread_bias(diag_ref, band_ref, x):
    tok, window = band_ref.shape
    line = diag_ref[pl.ds(x, 1), :]
    wide = jnp.broadcast_to(line, (tok, line.shape[1]))
    wide = pltpu.roll(wide, 0, 1, stride=1, stride_axis=0)[:, :window] * LOG2E
    qseg = lax.broadcasted_iota(jnp.int32, (tok, window), 0) // SEG
    kseg = lax.broadcasted_iota(jnp.int32, (tok, window), 1) // SEG
    band_ref[...] = jnp.where((kseg >= qseg) & (kseg <= qseg + LEFT), wide, NEG_FILL)


def attend(block, first_row, qs, ks, vs, band_ref):
    tok, window = band_ref.shape
    head = qs.shape[1]
    at = pl.multiple_of(block * tok, tok)
    query = qs[pl.ds(at, tok), :]
    keys = ks[pl.ds(at, window), :]
    values = vs[pl.ds(at, window), :]
    scores = lax.dot_general(query, keys, NT, preferred_element_type=F32)
    scores = scores * (head**-0.5 * LOG2E) + band_ref[...]
    if first_row is not None:
        column = lax.broadcasted_iota(jnp.int32, (1, window), 1) + block * tok
        hidden = jnp.logical_and(column < REACH, first_row)
        scores = scores + jnp.where(hidden, NEG_FILL, 0.0)
    largest = jnp.max(scores, axis=-1, keepdims=True)
    weights = jnp.exp2(scores - largest)
    total = jnp.sum(weights, axis=-1, keepdims=True)
    mixed = jnp.dot(weights.astype(BF), values, preferred_element_type=F32)
    return (mixed / total).astype(BF)


def attend_rows(side, x, y, qs, ks, vs, band, outs, mixed, ssem, rsem, halo_wait):
    tok, head = band.shape[0], qs.shape[1]
    here = pl.ds(pl.multiple_of(x * head, head), head)

    def hand_back(block):
        rows = pl.ds(pl.multiple_of(block * tok, tok), tok)
        return remote(
            outs.at[rows, :], mixed.at[:, here], ssem.at[block], rsem.at[x], sp=y * side + block
        )

    def run(block, first_row):
        result = attend(block, first_row, qs, ks, vs, band)
        outs[pl.ds(pl.multiple_of(block * tok, tok), tok), :] = result

        @pl.when(block != x)
        def _():
            hand_back(block).start()

        @pl.when(block == x)
        def _():
            mixed[:, here] = result

    half = REACH // tok

    def late(i, carry):
        run(i + half, None)
        return carry

    lax.fori_loop(0, side - half, late, 0)
    halo_wait()

    def early(i, carry):
        run(i, y == 0)
        return carry

    lax.fori_loop(0, half, early, 0)

    def finish(block, carry):
        @pl.when(block != x)
        def _():
            hand_back(block).wait_send()
            there = pl.ds(pl.multiple_of(block * head, head), head)
            remote(
                outs.at[pl.ds(0, tok), :],
                mixed.at[:, there],
                ssem.at[block],
                rsem.at[block],
                sp=y * side + block,
            ).wait_recv()

        return carry

    lax.fori_loop(0, side, finish, 0)


def clear_halo(y, ks, vs):
    @pl.when(y == 0)
    def _():
        ks[pl.ds(0, REACH), :] = jnp.zeros((REACH, ks.shape[1]), BF)
        vs[pl.ds(0, REACH), :] = jnp.zeros((REACH, vs.shape[1]), BF)


def first_kernel(
    side, q_ref, k_ref, v_ref, diag_ref, wq_ref, wk_ref, wv_ref, mixed_ref, wall_ref,
    qs, ks, vs, outs, mixed, wall, band, s_a2a, r_a2a, s_up, r_up, s_down, r_down,
    s_halo, r_halo, s_back, r_back,
):
    x, y, _ = place(side)
    tok, head = q_ref.shape[0], qs.shape[1]
    wrow = wq_ref.shape[0]
    group = side * wrow
    greet(side, x, y, True, False)

    mine = pl.ds(pl.multiple_of(x * tok, tok), tok)
    mine_late = pl.ds(pl.multiple_of(REACH + x * tok, tok), tok)
    wmine = pl.ds(pl.multiple_of(y * group + x * wrow, wrow), wrow)
    kinds = [
        (wq_ref, lambda: wall.at[wmine, pl.ds(0, head)]),
        (wk_ref, lambda: wall.at[wmine, pl.ds(head, head)]),
        (wv_ref, lambda: wall.at[wmine, pl.ds(2 * head, head)]),
        (k_ref, lambda: ks.at[mine_late, :]),
        (v_ref, lambda: vs.at[mine_late, :]),
        (q_ref, lambda: qs.at[mine, :]),
    ]

    def piece(kind, d):
        peer = lax.rem(x + d, side)
        src, dst = kinds[kind]
        cut = src.at[:, pl.ds(pl.multiple_of(peer * head, head), head)]
        if d == 0:
            return pltpu.make_async_copy(cut, dst(), r_a2a.at[kind, 0])
        return remote(cut, dst(), s_a2a.at[kind, d], r_a2a.at[kind, d], sp=y * side + peer)

    pieces = [[piece(kind, d) for d in range(side)] for kind in range(6)]
    for kind in range(6):
        for d in range(side):
            pieces[kind][d].start()

    def take(kind):
        pieces[kind][0].wait()
        for d in range(1, side):
            pieces[kind][d].wait_recv()

    up = lax.rem(y + 1, side) * side + x
    down = lax.rem(y + side - 1, side) * side + x

    def ring(step, going_up):
        owner = lax.rem(y - step + side, side) if going_up else lax.rem(y + step, side)
        rows = pl.ds(pl.multiple_of(owner * group, group), group)
        ss, rs = (s_up, r_up) if going_up else (s_down, r_down)
        return remote(
            wall.at[rows, :], wall.at[rows, :], ss.at[step], rs.at[step],
            sp=up if going_up else down,
        )

    ups, downs = side // 2, side // 2 - 1

    def relay(step):
        if 0 < step <= ups:
            ring(step - 1, True).wait_recv()
        if step < ups:
            ring(step, True).start()
        if 0 < step <= downs:
            ring(step - 1, False).wait_recv()
        if step < downs:
            ring(step, False).start()

    clear_halo(y, ks, vs)
    spread_bias(diag_ref, band, x)
    for kind in (0, 1, 2):
        take(kind)
    relay(0)
    for kind in (3, 4):
        take(kind)

    late = pl.ds(REACH + side * tok - REACH, REACH)
    halo = [
        remote(a.at[late, :], a.at[pl.ds(0, REACH), :], s_halo.at[i], r_halo.at[i], sp=up)
        for i, a in enumerate((ks, vs))
    ]

    @pl.when(y < side - 1)
    def _():
        for copy in halo:
            copy.start()

    relay(1)
    take(5)

    def halo_wait():
        relay(2)

        @pl.when(y > 0)
        def _():
            for copy in halo:
                copy.wait_recv()

    attend_rows(side, x, y, qs, ks, vs, band, outs, mixed, s_back, r_back, halo_wait)
    for step in range(3, ups + 1):
        relay(step)
    mixed_ref[...] = mixed[...]
    wall_ref[...] = wall[...]

    for kind in range(6):
        for d in range(1, side):
            pieces[kind][d].wait_send()
    for step in range(ups):
        ring(step, True).wait_send()
    for step in range(downs):
        ring(step, False).wait_send()

    @pl.when(y < side - 1)
    def _():
        for copy in halo:
            copy.wait_send()


def project(mixed_ref, w_any, wbuf, wsem, part, cuts):
    n = w_any.shape[0] // cuts
    loads = [
        pltpu.make_async_copy(
            w_any.at[pl.ds(i * n, n), :], wbuf.at[pl.ds(i * n, n), :], wsem.at[i]
        )
        for i in range(cuts)
    ]
    for load in loads:
        load.start()

    def piece(i):
        loads[i].wait()
        done = lax.dot_general(
            mixed_ref[...], wbuf[pl.ds(i * n, n), :], NT, preferred_element_type=F32
        )
        part[:, pl.ds(i * n, n)] = done.astype(BF)

    return piece, n


CUTS = 4


def second_kernel(
    side, mixed_ref, w_any, resid_any, post_ref, pre_ref, wall_ref, diag_ref, out_ref, hid_ref,
    wbuf, part, theirs, resid, inp, qs, ks, vs, outs, mixed, band, wsem, rsem,
    s_part, r_part, s_right, r_right, s_left, r_left, s_d2d, r_d2d, s_halo, r_halo,
    s_back, r_back, s_hid, r_hid, hid,
):
    x, y, c = place(side)
    tok = mixed_ref.shape[0]
    head = qs.shape[1]
    half = tok // 2
    chunk = half // 2
    other = 1 - c
    load_resid = pltpu.make_async_copy(
        resid_any.at[pl.ds(pl.multiple_of(c * half, half), half), :], resid, rsem.at[0]
    )
    piece, n = project(mixed_ref, w_any, wbuf, wsem, part, CUTS)
    load_resid.start()
    greet(side, x, y, True, True)

    swaps = [
        remote(
            part.at[pl.ds(pl.multiple_of(other * half, half), half), pl.ds(i * n, n)],
            theirs.at[:, pl.ds(i * n, n)],
            s_part.at[i],
            r_part.at[i],
            tp=other,
        )
        for i in range(CUTS)
    ]
    for i in range(CUTS):
        piece(i)
        swaps[i].start()
    clear_halo(y, ks, vs)
    spread_bias(diag_ref, band, x)
    load_resid.wait()
    for copy in swaps:
        copy.wait_recv()

    def rows_of(owner, core, r):
        return pl.ds(pl.multiple_of(owner * tok + core * half + r * chunk, chunk), chunk)

    right = y * side + lax.rem(x + 1, side)
    left = y * side + lax.rem(x + side - 1, side)

    def owner_right(step):
        return lax.rem(x - step + side, side)

    def owner_left(step):
        return lax.rem(x + step, side)

    def pass_right(step, r):
        rows = rows_of(owner_right(step), c, r)
        return remote(
            inp.at[rows, :], inp.at[rows, :], s_right.at[step, r], r_right.at[step, r], sp=right
        )

    def pass_left(step, r):
        rows = rows_of(owner_left(step), c, r)
        return remote(
            inp.at[rows, :], inp.at[rows, :], s_left.at[step, r], r_left.at[step, r], sp=left
        )

    def share(owner, slot, r, core):
        rows = rows_of(owner, core, r)
        return remote(
            inp.at[rows, :], inp.at[rows, :], s_d2d.at[slot, r], r_d2d.at[slot, r], tp=other
        )

    def send_hid(r):
        rows = pl.ds(pl.multiple_of(c * half + r * chunk, chunk), chunk)
        return remote(hid.at[rows, :], hid.at[rows, :], s_hid.at[r], r_hid.at[r], tp=other)

    last = side // 2 - 1
    for r in range(2):
        rows = pl.ds(pl.multiple_of(c * half + r * chunk, chunk), chunk)
        sub = pl.ds(r * chunk, chunk)
        branch = part[rows, :].astype(F32) + theirs[sub, :].astype(F32)
        branch = branch.astype(BF).astype(F32)
        scale = lax.rsqrt(jnp.mean(branch * branch, axis=-1, keepdims=True) + EPS)
        hidden = (resid[sub, :].astype(F32) + branch * scale * post_ref[...]).astype(BF)
        hid[rows, :] = hidden
        wide = hidden.astype(F32)
        scale = lax.rsqrt(jnp.mean(wide * wide, axis=-1, keepdims=True) + EPS)
        inp[rows_of(x, c, r), :] = (wide * scale * pre_ref[...]).astype(BF)
        pass_right(0, r).start()
        pass_left(0, r).start()
        share(x, 0, r, c).start()
        send_hid(r).start()

    up = lax.rem(y + 1, side) * side + x
    shift = REACH // tok

    def halo(owner):
        slot = owner - (side - shift)
        rows = pl.ds(pl.multiple_of(REACH + owner * tok, tok), tok)
        dest = pl.ds(pl.multiple_of(slot * tok, tok), tok)
        return [
            remote(a.at[rows, :], a.at[dest, :], s_halo.at[i, slot], r_halo.at[i, slot], sp=up)
            for i, a in enumerate((ks, vs))
        ]

    def qkv(owner):
        rows = pl.ds(pl.multiple_of(owner * tok, tok), tok)
        late = pl.ds(pl.multiple_of(REACH + owner * tok, tok), tok)
        done = jnp.dot(inp[rows, :], wall_ref[...], preferred_element_type=F32).astype(BF)
        qs[rows, :] = done[:, :head]
        ks[late, :] = done[:, head : 2 * head]
        vs[late, :] = done[:, 2 * head :]

        @pl.when(jnp.logical_and(owner >= side - shift, y < side - 1))
        def _():
            for copy in halo(owner):
                copy.start()

    for r in range(2):
        share(x, 0, r, other).wait_recv()
    qkv(x)
    for step in range(1, last + 1):
        for r in range(2):
            rows = rows_of(owner_right(step), c, r)
            remote(
                inp.at[rows, :], inp.at[rows, :], s_right.at[step - 1, r],
                r_right.at[step - 1, r], sp=right,
            ).wait_recv()
            if not (step == last and r == 1):
                pass_right(step, r).start()
            share(owner_right(step), step, r, c).start()
            rows = rows_of(owner_left(step), c, r)
            remote(
                inp.at[rows, :], inp.at[rows, :], s_left.at[step - 1, r],
                r_left.at[step - 1, r], sp=left,
            ).wait_recv()
            if not (step == last and r == 0):
                pass_left(step, r).start()
            share(owner_left(step), last + 1 + step, r, c).start()
        for r in range(2):
            share(owner_right(step), step, r, other).wait_recv()
        qkv(owner_right(step))
        for r in range(2):
            share(owner_left(step), last + 1 + step, r, other).wait_recv()
        qkv(owner_left(step))
    far = lax.rem(x + side // 2, side)
    step = last + 1
    rows = rows_of(far, c, 0)
    remote(
        inp.at[rows, :], inp.at[rows, :], s_right.at[last, 0], r_right.at[last, 0], sp=right
    ).wait_recv()
    share(far, step, 0, c).start()
    rows = rows_of(far, c, 1)
    remote(
        inp.at[rows, :], inp.at[rows, :], s_left.at[last, 1], r_left.at[last, 1], sp=left
    ).wait_recv()
    share(far, step, 1, c).start()
    for r in range(2):
        share(far, step, r, other).wait_recv()
    qkv(far)

    def halo_wait():
        @pl.when(y > 0)
        def _():
            for k in range(shift):
                for copy in halo(side - shift + k):
                    copy.wait_recv()

    attend_rows(side, x, y, qs, ks, vs, band, outs, mixed, s_back, r_back, halo_wait)
    out_ref[...] = mixed[...]
    for r in range(2):
        rows = pl.ds(pl.multiple_of(other * half + r * chunk, chunk), chunk)
        remote(hid.at[rows, :], hid.at[rows, :], s_hid.at[r], r_hid.at[r], tp=other).wait_recv()
    hid_ref[...] = hid[...]

    for copy in swaps:
        copy.wait_send()
    for step in range(last + 1):
        for r in range(2):
            if not (step == last and r == 1):
                pass_right(step, r).wait_send()
            if not (step == last and r == 0):
                pass_left(step, r).wait_send()
    for r in range(2):
        send_hid(r).wait_send()
        share(x, 0, r, c).wait_send()
        share(far, last + 1, r, c).wait_send()
        for step in range(1, last + 1):
            share(owner_right(step), step, r, c).wait_send()
            share(owner_left(step), last + 1 + step, r, c).wait_send()

    @pl.when(y < side - 1)
    def _():
        for k in range(shift):
            for copy in halo(side - shift + k):
                copy.wait_send()


def third_kernel(
    side, mixed_ref, w_any, hid_ref, post_ref, out_ref, wbuf, part, theirs, wsem, s_part, r_part
):
    x, y, c = place(side)
    piece, n = project(mixed_ref, w_any, wbuf, wsem, part, CUTS)
    greet(side, x, y, False, True)
    swaps = [
        remote(
            part.at[:, pl.ds(i * n, n)],
            theirs.at[:, pl.ds(i * n, n)],
            s_part.at[i],
            r_part.at[i],
            tp=1 - c,
        )
        for i in range(CUTS)
    ]
    for i in range(CUTS):
        piece(i)
        swaps[i].start()
    for copy in swaps:
        copy.wait_recv()
    rows = 32
    for r in range(part.shape[0] // rows):
        sub = pl.ds(r * rows, rows)
        branch = part[sub, :].astype(F32) + theirs[sub, :].astype(F32)
        branch = branch.astype(BF).astype(F32)
        scale = lax.rsqrt(jnp.mean(branch * branch, axis=-1, keepdims=True) + EPS)
        out_ref[sub, :] = (hid_ref[sub, :].astype(F32) + branch * scale * post_ref[...]).astype(BF)
    for copy in swaps:
        copy.wait_send()


def diagonals(table, tok):
    window = tok + REACH
    far = table[:, 2 * REL_CLIP :]
    heads = table.shape[0]
    before = jnp.broadcast_to(far, (heads, REACH - REL_CLIP))
    near = table[:, :0:-1]
    after = jnp.broadcast_to(far, (heads, window + tok - REACH - REL_CLIP))
    return jnp.concatenate([before, near, after], axis=1)


def shards(
    side, resid, queries_first, keys_first, values_first, rel_first, post_first, out_first,
    pre_second, query_weight, key_weight, value_weight, rel_second, post_second, out_second,
):
    tok, width = queries_first.shape
    model = resid.shape[1]
    heads = rel_first.shape[0]
    head = width // heads
    rows = side * tok
    dma = pltpu.SemaphoreType.DMA
    params = functools.partial(pltpu.CompilerParams, has_side_effects=True)

    def shape(*dims):
        return jax.ShapeDtypeStruct(dims, BF)

    def vmem(*dims):
        return pltpu.VMEM(dims, BF)

    w_first = lax.all_gather(out_first.T, "sp", axis=0, tiled=True)
    w_second = lax.all_gather(out_second.T, "sp", axis=0, tiled=True)
    attention = [
        vmem(rows, head),
        vmem(rows + REACH, head),
        vmem(rows + REACH, head),
        vmem(rows, head),
        vmem(tok, width),
    ]
    band = pltpu.VMEM((tok, tok + REACH), F32)
    steps = side // 2
    mixed, wall = pl.pallas_call(
        functools.partial(first_kernel, side),
        out_shape=(shape(tok, width), shape(model, 3 * head)),
        in_specs=[ANY] * 3 + [VM] + [ANY] * 3,
        out_specs=(VM, VM),
        scratch_shapes=attention
        + [vmem(model, 3 * head), band]
        + [dma((6, side))] * 2
        + [dma((steps,))] * 4
        + [dma((2,))] * 2
        + [dma((side,))] * 2,
        compiler_params=params(collective_id=0),
        cost_estimate=pl.CostEstimate(
            flops=20_000_000_000, bytes_accessed=4_000_000, transcendentals=0
        ),
    )(
        queries_first,
        keys_first,
        values_first,
        diagonals(rel_first, tok),
        query_weight,
        key_weight,
        value_weight,
    )
    mixed, hidden = pl.pallas_call(
        functools.partial(second_kernel, side),
        out_shape=(shape(tok, width), shape(tok, model)),
        in_specs=[VM, ANY, ANY, VM, VM, VM, VM],
        out_specs=(VM, VM),
        scratch_shapes=[
            vmem(model, width),
            vmem(tok, model),
            vmem(tok // 2, model),
            vmem(tok // 2, model),
            vmem(rows, model),
        ]
        + attention
        + [band]
        + [dma((CUTS,)), dma((1,))]
        + [dma((CUTS,))] * 2
        + [dma((steps, 2))] * 4
        + [dma((side, 2))] * 2
        + [dma((2, REACH // tok))] * 2
        + [dma((side,))] * 2
        + [dma((2,))] * 2
        + [vmem(tok, model)],
        compiler_params=params(collective_id=1),
        cost_estimate=pl.CostEstimate(
            flops=30_000_000_000, bytes_accessed=8_000_000, transcendentals=0
        ),
    )(
        mixed,
        w_first,
        resid,
        post_first[None],
        pre_second[None],
        wall,
        diagonals(rel_second, tok),
    )
    return pl.pallas_call(
        functools.partial(third_kernel, side),
        out_shape=shape(tok, model),
        in_specs=[VM, ANY, VM, VM],
        out_specs=VM,
        scratch_shapes=[vmem(model, width), vmem(tok, model), vmem(tok, model)]
        + [dma((CUTS,))] * 3,
        compiler_params=params(collective_id=2),
        cost_estimate=pl.CostEstimate(
            flops=5_000_000_000, bytes_accessed=5_000_000, transcendentals=0
        ),
    )(mixed, w_second, hidden, post_second[None])


def solution(mesh):
    side = math.isqrt(mesh.shape["sp"])
    in_specs = (
        P(("grp", "sp"), None),
        P(("grp", "sp"), "tp"),
        P(("grp", "sp"), "tp"),
        P(("grp", "sp"), "tp"),
        P("tp", None),
        P(),
        P("tp", "sp"),
        P(),
        P("sp", "tp"),
        P("sp", "tp"),
        P("sp", "tp"),
        P("tp", None),
        P(),
        P("tp", "sp"),
    )
    out_specs = P(("grp", "sp"), None)
    return jax.shard_map(
        functools.partial(shards, side),
        mesh=mesh,
        in_specs=in_specs,
        out_specs=out_specs,
        check_vma=False,
    )
```

time: 418 us -> 217 us (0.52)
  waiting for transfers between devices: 231 us -> 72.7 us
  Pallas kernels: 0 us -> 124 us
  starting transfers between devices: 84.9 us -> 0.06 us
  matrix products: 38.3 us -> 0 us
  local copies, waits for them, and re-layouts: 27.8 us -> 5.62 us
  blocking collectives: 16 us -> 0 us
    pallas_call x0 -> x3, Pallas kernels: none -> 124 us  [the longest x1 59.4 us: shards(): pl.pallas_call(functools.partial(first_kernel, side), out_shape=(shape(to...]
    ppermute x16 -> x0, waiting for transfers between devices: 98.4 us -> none  [from_behind(): lax.ppermute(value, axis, [(source, source + steps) for source in range(i...]
    ppermute x16 -> x0, starting transfers between devices: 84.8 us -> none  [from_behind(): lax.ppermute(value, axis, [(source, source + steps) for source in range(i...]
    all_gather x3 -> x2, waiting for transfers between devices: 132 us -> 71.2 us  [the longest x1 37.5 us: shards(): w_first = lax.all_gather(out_first.T, 'sp', axis=0, tiled=True)]
    dot_general x11 -> x0, matrix products: 33.2 us -> none  [the longest x2 9.85 us: attend_band(): jnp.einsum('nhqk,nkhd->nqhd', weights, value_band, preferred_element_type...]
    unnamed x96 -> x1, local copies, waits for them, and re-layouts: 21.1 us -> 1.88 us
    all_to_all x2 -> x0, blocking collectives: 16 us -> none  [sent_to_all(): return lax.all_to_all(copies, axis, split_axis=0, concat_axis=0, tiled=True)]
    sub x2 -> x0, matrix products: 5.07 us -> none  [attend_band(): weights = jnp.exp(scores - largest)]
  transfers between devices with their start and end apart: 19 -> 2, of which waited for: 11 -> 2; matrix products, arithmetic and copies ran while one was open for 15% -> 2% of each run, Pallas kernels for 0% -> 52%
where the time goes in v1:
time: 217 us
  Pallas kernels  124 us (57%)
  waiting for transfers between devices  72.7 us (34%)
  between operations  13.5 us (6%)
  local copies, waits for them, and re-layouts  5.62 us (3%)
    pallas_call x1, Pallas kernels, shards(): pl.pallas_call(functools.partial(first_kernel, side), out_shape=(shape(to...  59.4 us
    pallas_call x1, Pallas kernels, shards(): pl.pallas_call(functools.partial(second_kernel, side), out_shape=(shape(t...  52.7 us
    all_gather x1, waiting for transfers between devices, shards(): w_first = lax.all_gather(out_first.T, 'sp', axis=0, tiled=True)  37.5 us
    all_gather x1, waiting for transfers between devices, shards(): w_second = lax.all_gather(out_second.T, 'sp', axis=0, tiled=True)  33.7 us
    pallas_call x1, Pallas kernels, shards(): pl.pallas_call(functools.partial(third_kernel, side), out_shape=shape(tok...  11.8 us
  transfers between devices with their start and end apart: 2, of which 2 were waited for; matrix products, arithmetic and copies ran while one was open for 2% of the time, Pallas kernels for 52%

profile of v1, /device:TPU:513, one launch (start us, length us, event | category | flops | bytes accessed | tf_op | source)
XLA Modules:
  0.0 217.0 jit_solution(7449876653162796442)
XLA Ops:
  6.5 0.0 all-gather.3.cloned.1.call-start
  6.6 0.7 all-gather.3.cloned.1.call-update
  7.3 0.1 all-gather.5.cloned.1.call-start
  7.4 0.7 all-gather.5.cloned.1.call-update
  8.1 0.8 slice.13
  8.9 0.1 rev.6
  9.0 0.8 slice.15
  9.8 0.1 rev.7
  10.0 0.8 slice_reduce_fusion.1
  10.8 0.8 slice_reduce_fusion
  11.6 0.1 broadcast_in_dim.34
  11.6 0.1 broadcast_in_dim.35
  11.7 0.6 pad_maximum_fusion.diag_ref
  12.3 0.1 broadcast_in_dim.39
  12.4 0.1 broadcast_in_dim.40
  12.5 0.6 pad_maximum_fusion.1.diag_ref
  13.1 59.4 %shard_map.136 = (bf16[128,1024]{1,0:T(8,128)(2,1)}, bf16[2048,384]{1,0:T(8,128)(2,1)}) custom-call(bf16[128,1024]{1,0:T(8,128)(2,1)} %q_ref.1, bf16[128,1024]{1,0:T(8,128)(2,1)} %k_ref.1, bf16[128,1024]{1,0:T(8,128)(2,1)} %v_ref.1, f32[8,768]{1,0:T(8,128)} %pad_maximum_fusion.diag_ref, bf16[32,1024]{1,0:T(8,128)(2,1)} %wq_ref.1, bf16[32,1024]{1,0:T(8,128)(2,1)} %wk_ref.1, ...), custom_call_target="tpu_custom_call" | custom-call | flops 20000000000 | bytes 4000000 | tf_op jit(solution)/shard_map/pallas_call | solution.py:558
  72.5 37.5 %all-gather.3.cloned.1.call-done.w_any = bf16[2048,1024]{1,0:T(8,128)(2,1)} async-done(((bf16[32,1024]{1,0:T(8,128)(2,1)}), bf16[2048,1024]{1,0:T(8,128)(2,1)}) %all-gather.3.cloned.1.call-update) | async-done | bytes 4194320 | tf_op jit(solution)/shard_map/all_gather | solution.py:547
  110.0 52.7 %shard_map.137 = (bf16[128,1024]{1,0:T(8,128)(2,1)}, bf16[128,2048]{1,0:T(8,128)(2,1)}) custom-call(bf16[128,1024]{1,0:T(8,128)(2,1)} %get-tuple-element.9.mixed_ref, bf16[2048,1024]{1,0:T(8,128)(2,1)} %all-gather.3.cloned.1.call-done.w_any, bf16[128,2048]{1,0:T(8,128)(2,1)} %resid_any.1, f32[1,2048]{1,0:T(1,128)} %bitcast.7, f32[1,2048]{1,0:T(1,128)} %bitcast.8, ...), custom_call_target="tpu_custom_call" | custom-call | flops 30000001024 | bytes 8000000 | tf_op jit(solution)/shard_map/pallas_call | solution.py:582
  162.8 33.7 %all-gather.5.cloned.1.call-done.w_any = bf16[2048,1024]{1,0:T(8,128)(2,1)} async-done(((bf16[32,1024]{1,0:T(8,128)(2,1)}), bf16[2048,1024]{1,0:T(8,128)(2,1)}) %all-gather.5.cloned.1.call-update) | async-done | bytes 4194320 | tf_op jit(solution)/shard_map/all_gather | solution.py:548
  196.5 11.8 %shard_map.138 = bf16[128,2048]{1,0:T(8,128)(2,1)} custom-call(bf16[128,1024]{1,0:T(8,128)(2,1)} %get-tuple-element.11.mixed_ref, bf16[2048,1024]{1,0:T(8,128)(2,1)} %all-gather.5.cloned.1.call-done.w_any, bf16[128,2048]{1,0:T(8,128)(2,1)} %get-tuple-element.12.hid_ref, f32[1,2048]{1,0:T(1,128)} %bitcast.9), custom_call_target="tpu_custom_call" | custom-call | flops 5000000000 | bytes 5000000 | tf_op jit(solution)/shard_map/pallas_call | solution.py:617
  208.2 1.9 copy.16
Async XLA Ops:
  6.5 103.5 %all-gather.3.cloned.1.call-start = ((), (), s32[]{:S(2)}) async-start(), calls=%async_computation | async-start | bytes 4259840 | tf_op jit(solution)/shard_map/all_gather | solution.py:547
  7.3 189.2 %all-gather.5.cloned.1.call-start = ((), (), s32[]{:S(2)}) async-start(), calls=%async_computation.1 | async-start | bytes 4259840 | tf_op jit(solution)/shard_map/all_gather | solution.py:548
Sparse Core Ops, SparseCore 0:
  9.9 100.1 all-gather.2
  112.5 83.8 all-gather.4

commit v2 on v0

v2 whole, which is shorter than its diff:
```python
import functools
import math

import jax
import jax.numpy as jnp
from jax import lax
from jax.experimental import pallas as pl
from jax.experimental.pallas import tpu as pltpu
from jax.sharding import PartitionSpec as P

SEG = 64
LEFT = 8
REACH = 512
REL_CLIP = 128
EPS = 1e-06
NEG_FILL = -1e30
LOG2E = 1.4426950408889634
BF = jnp.bfloat16
F32 = jnp.float32
MESH = pl.DeviceIdType.MESH
VM = pl.BlockSpec(memory_space=pltpu.VMEM)
ANY = pl.BlockSpec(memory_space=pl.ANY)
NT = (((1,), (1,)), ((), ()))


def place(side):
    sp = lax.axis_index("sp")
    return lax.rem(sp, side), lax.div(sp, side), lax.axis_index("tp")


def remote(src, dst, send, recv, **where):
    return pltpu.make_async_remote_copy(
        src_ref=src,
        dst_ref=dst,
        send_sem=send,
        recv_sem=recv,
        device_id=dict(where),
        device_id_type=MESH,
    )


def greet(side, x, y, c, grp):
    barrier = pltpu.get_barrier_semaphore()
    peers = [{"sp": y * side + lax.rem(x + d, side)} for d in range(1, side)]
    peers += [{"sp": lax.rem(y + d, side) * side + x} for d in (1, side - 1)]
    peers += [{"tp": 1 - c}, {"grp": other_plane(grp)}]
    for peer in peers:
        pl.semaphore_signal(barrier, inc=1, device_id=peer, device_id_type=MESH)
    return lambda: pl.semaphore_wait(barrier, len(peers))


def other_plane(grp):
    return grp + 1 - 2 * lax.rem(grp, 2)


def spread_bias(table_ref, band_ref, x):
    tok, window = band_ref.shape
    length = window + tok
    near = table_ref[:, : 2 * REL_CLIP]
    far = table_ref[:, 2 * REL_CLIP :]
    end = REACH + REL_CLIP
    slot = end - lax.broadcasted_iota(jnp.int32, (2 * REL_CLIP, length), 1)
    pick = slot == lax.broadcasted_iota(jnp.int32, (2 * REL_CLIP, length), 0)
    lines = jnp.dot(
        near, pick.astype(F32), preferred_element_type=F32, precision=lax.Precision.HIGHEST
    )
    where = lax.broadcasted_iota(jnp.int32, lines.shape, 1)
    lines = jnp.where((where > end - 2 * REL_CLIP) & (where < end), lines, far)
    chosen = lax.broadcasted_iota(jnp.int32, lines.shape, 0) == x
    line = jnp.sum(jnp.where(chosen, lines, 0.0), axis=0, keepdims=True)
    wide = jnp.broadcast_to(line, (tok, length))
    wide = pltpu.roll(wide, 0, 1, stride=1, stride_axis=0)[:, :window] * LOG2E
    qseg = lax.broadcasted_iota(jnp.int32, (tok, window), 0) // SEG
    kseg = lax.broadcasted_iota(jnp.int32, (tok, window), 1) // SEG
    band_ref[...] = jnp.where((kseg >= qseg) & (kseg <= qseg + LEFT), wide, NEG_FILL)


def attend(block, first_row, qs, ks, vs, band_ref):
    tok, window = band_ref.shape
    head = qs.shape[1]
    at = pl.multiple_of(block * tok, tok)
    query = qs[pl.ds(at, tok), :]
    keys = ks[pl.ds(at, window), :]
    values = vs[pl.ds(at, window), :]
    scores = lax.dot_general(query, keys, NT, preferred_element_type=F32)
    scores = scores * (head**-0.5 * LOG2E) + band_ref[...]
    if first_row is not None:
        column = lax.broadcasted_iota(jnp.int32, (1, window), 1) + block * tok
        hidden = jnp.logical_and(column < REACH, first_row)
        scores = scores + jnp.where(hidden, NEG_FILL, 0.0)
    largest = jnp.max(scores, axis=-1, keepdims=True)
    weights = jnp.exp2(scores - largest)
    total = jnp.sum(weights, axis=-1, keepdims=True)
    mixed = jnp.dot(weights.astype(BF), values, preferred_element_type=F32)
    return (mixed / total).astype(BF)


def attend_rows(side, x, y, qs, ks, vs, band, outs, mixed, ssem, rsem, between):
    tok, head = band.shape[0], qs.shape[1]
    here = pl.ds(pl.multiple_of(x * head, head), head)

    def hand_back(block):
        rows = pl.ds(pl.multiple_of(block * tok, tok), tok)
        return remote(
            outs.at[rows, :], mixed.at[:, here], ssem.at[block], rsem.at[x], sp=y * side + block
        )

    def run(block, first_row):
        result = attend(block, first_row, qs, ks, vs, band)
        outs[pl.ds(pl.multiple_of(block * tok, tok), tok), :] = result

        @pl.when(block != x)
        def _():
            hand_back(block).start()

        @pl.when(block == x)
        def _():
            mixed[:, here] = result

    half = REACH // tok

    def late(i, carry):
        run(i + half, None)
        return carry

    lax.fori_loop(0, side - half, late, 0)
    between()

    def early(i, carry):
        run(i, y == 0)
        return carry

    lax.fori_loop(0, half, early, 0)

    def take_back():
        def finish(block, carry):
            @pl.when(block != x)
            def _():
                there = pl.ds(pl.multiple_of(block * head, head), head)
                remote(
                    outs.at[pl.ds(0, tok), :],
                    mixed.at[:, there],
                    ssem.at[block],
                    rsem.at[block],
                    sp=y * side + block,
                ).wait_recv()

            return carry

        lax.fori_loop(0, side, finish, 0)

    def sent():
        def finish(block, carry):
            @pl.when(block != x)
            def _():
                hand_back(block).wait_send()

            return carry

        lax.fori_loop(0, side, finish, 0)

    return take_back, sent


def clear_halo(y, ks, vs):
    @pl.when(y == 0)
    def _():
        ks[pl.ds(0, REACH), :] = jnp.zeros((REACH, ks.shape[1]), BF)
        vs[pl.ds(0, REACH), :] = jnp.zeros((REACH, vs.shape[1]), BF)


class Gather:
    def __init__(self, side, x, y, grp, buf, xr, xl, yu, yd, z):
        self.side, self.x, self.y, self.grp, self.buf = side, x, y, grp, buf
        self.xr, self.xl, self.yu, self.yd, self.z = xr, xl, yu, yd, z
        self.rows = buf.shape[0] // (side * side)
        quarter = buf.shape[1] // 4
        parity = lax.rem(grp, 2)
        self.inside = pl.ds(pl.multiple_of(parity * quarter, quarter), 3 * quarter)
        self.across = pl.ds(pl.multiple_of(parity * 3 * quarter, quarter), quarter)
        self.theirs = pl.ds(pl.multiple_of((1 - parity) * 3 * quarter, quarter), quarter)

    def slab(self, xp, yp, columns):
        at = pl.multiple_of((yp * self.side + xp) * self.rows, self.rows)
        return self.buf.at[pl.ds(at, self.rows), columns]

    def column(self, k):
        if isinstance(k, int):
            off = -(k + 1) // 2 if k % 2 else k // 2
        else:
            off = jnp.where(lax.rem(k, 2) == 1, -lax.div(k + 1, 2), lax.div(k, 2))
        return lax.rem(self.x + off + self.side, self.side)

    def xcopy(self, step, right):
        owner = lax.rem(self.x + (-step if right else step) + self.side, self.side)
        to = lax.rem(self.x + (1 if right else self.side - 1), self.side)
        part = self.slab(owner, self.y, self.inside)
        send, recv = self.xr if right else self.xl
        return remote(part, part, send.at[step], recv.at[step], sp=self.y * self.side + to)

    def xarrival(self, step, right):
        owner = lax.rem(self.x + (-step - 1 if right else step + 1) + self.side, self.side)
        part = self.slab(owner, self.y, self.inside)
        send, recv = self.xr if right else self.xl
        return remote(part, part, send.at[step], recv.at[step], sp=self.y * self.side + self.x)

    def ycopy(self, step, k, upward):
        owner = lax.rem(self.y + (-step if upward else step) + self.side, self.side)
        to = lax.rem(self.y + (1 if upward else self.side - 1), self.side)
        part = self.slab(self.column(k), owner, self.inside)
        send, recv = self.yu if upward else self.yd
        return remote(part, part, send.at[step, k], recv.at[step, k], sp=to * self.side + self.x)

    def yarrival(self, step, k, upward):
        owner = lax.rem(self.y + (-step - 1 if upward else step + 1) + self.side, self.side)
        part = self.slab(self.column(k), owner, self.inside)
        send, recv = self.yu if upward else self.yd
        return remote(part, part, send.at[step, k], recv.at[step, k], sp=self.x)

    def zcopy(self, t, k, columns):
        owner = lax.rem(self.y - t + self.side, self.side)
        part = self.slab(self.column(k), owner, columns)
        send, recv = self.z
        return remote(part, part, send.at[t, k], recv.at[t, k], grp=other_plane(self.grp))

    def begin(self):
        self.xcopy(0, True).start()
        self.xcopy(0, False).start()
        self.ycopy(0, 0, True).start()
        self.ycopy(0, 0, False).start()

    def xevent(self, k):
        right = k % 2 == 1
        step = (k + 1) // 2 if right else k // 2
        self.xarrival(step - 1, right).wait_recv()
        if step < self.side // 2 - (0 if right else 1):
            self.xcopy(step, right).start()
        self.ycopy(0, k, True).start()
        self.ycopy(0, k, False).start()
        self.zcopy(0, k, self.across).start()

    def yevent(self, step, lower):
        side = self.side
        half = side // 2
        far = step == half
        base = 0 if lower else half

        def one(k, carry):
            if not far or lower:
                self.yarrival(step - 1, k, True).wait_recv()
                if step < half - 1 or (step == half - 1 and lower):
                    self.ycopy(step, k, True).start()
                self.zcopy(step, k, self.across).start()
            if not far or not lower:
                self.yarrival(step - 1, k, False).wait_recv()
                if step < half - 1 or (step == half - 1 and not lower):
                    self.ycopy(step, k, False).start()
                self.zcopy(side - step, k, self.across).start()
            return carry

        lax.fori_loop(base, base + half, one, 0)

    def zevent(self):
        side = self.side

        def one(i, carry):
            t, k = lax.div(i, side), lax.rem(i, side)
            self.zcopy(t, k, self.theirs).wait_recv()
            return carry

        lax.fori_loop(1, side * side, one, 0)

    def sent(self):
        side = self.side
        half = side // 2
        for step in range(half):
            self.xcopy(step, True).wait_send()
            if step < half - 1:
                self.xcopy(step, False).wait_send()

            def one(k, carry, step=step):
                if step < half - 1:
                    self.ycopy(step, k, True).wait_send()
                    self.ycopy(step, k + half, True).wait_send()
                    self.ycopy(step, k, False).wait_send()
                else:
                    self.ycopy(step, k, True).wait_send()
                self.ycopy(step, k + half, False).wait_send()
                return carry

            lax.fori_loop(0, half, one, 0)

        def one(i, carry):
            self.zcopy(lax.div(i, side), lax.rem(i, side), self.across).wait_send()
            return carry

        lax.fori_loop(1, side * side, one, 0)


CUTS = 4


def layers_kernel(side, names, *refs):
    r = dict(zip(names, refs))
    x, y, c = place(side)
    grp = lax.axis_index("grp")
    plane = lax.rem(grp, 2)
    q_ref, k_ref, v_ref = r["q"], r["k"], r["v"]
    tok, width = q_ref.shape
    head = width // side
    wall = r["wall"]
    wrow = r["wq"].shape[0]
    group = side * wrow
    model = r["w1"].shape[0]
    other = 1 - c
    half = tok // 2
    steps = side // 2
    up = lax.rem(y + 1, side) * side + x
    down = lax.rem(y + side - 1, side) * side + x
    right = y * side + lax.rem(x + 1, side)
    left = y * side + lax.rem(x + side - 1, side)

    meet = greet(side, x, y, c, grp)
    own = pl.ds(pl.multiple_of((y * side + x) * wrow, wrow), wrow)
    loads = [
        pltpu.make_async_copy(r["o1"], r["w1"].at[own, :], r["loads"].at[0]),
        pltpu.make_async_copy(r["o2"], r["w2"].at[own, :], r["loads"].at[1]),
        pltpu.make_async_copy(
            r["resid_any"].at[pl.ds(pl.multiple_of(c * half, half), half), :],
            r["resid"],
            r["loads"].at[2],
        ),
    ]
    for load in loads:
        load.start()
    g1, g2 = [
        Gather(
            side, x, y, grp, r[f"w{i}"],
            *((r[f"s{kind}{i}"], r[f"r{kind}{i}"]) for kind in ("xr", "xl", "yu", "yd", "z")),
        )
        for i in (1, 2)
    ]

    mine = pl.ds(pl.multiple_of(x * tok, tok), tok)
    mine_late = pl.ds(pl.multiple_of(REACH + x * tok, tok), tok)
    kinds = [
        (k_ref, r["ks1"].at[mine_late, :]),
        (v_ref, r["vs1"].at[mine_late, :]),
        (q_ref, r["qs1"].at[mine, :]),
    ] + [(r[f"w{n}"], wall.at[own, pl.ds(i * head, head)]) for i, n in enumerate("qkv")]

    def piece(kind, d):
        peer = lax.rem(x + d, side)
        src, dst = kinds[kind]
        cut = src.at[:, pl.ds(pl.multiple_of(peer * head, head), head)]
        if d == 0:
            return pltpu.make_async_copy(cut, dst, r["ra2a"].at[kind, 0])
        send, recv = r["sa2a"].at[kind, d], r["ra2a"].at[kind, d]
        return remote(cut, dst, send, recv, sp=y * side + peer)

    for kind in range(3):
        piece(kind, 0).start()
    in_plane = lax.div(x, steps) == plane

    @pl.when(in_plane)
    def _():
        for kind in range(3, 6):
            piece(kind, 0).start()

    spread_bias(r["rel1"], r["band1"], x)
    spread_bias(r["rel2"], r["band2"], x)
    clear_halo(y, r["ks1"], r["vs1"])
    clear_halo(y, r["ks2"], r["vs2"])
    for load in loads:
        load.wait()
    meet()

    g1.begin()
    near, wide = [1, side - 1, 2, side - 2], [3, side - 3, 4]
    for d in near:
        piece(0, d).start()
        piece(1, d).start()
    g1.xevent(1)
    g1.xevent(2)
    for d in wide:
        piece(0, d).start()
        piece(1, d).start()
    g1.xevent(3)
    g1.xevent(4)
    for d in near:
        piece(2, d).start()
    g1.xevent(5)
    g1.xevent(6)
    for d in wide:
        piece(2, d).start()

    @pl.when(in_plane)
    def _():
        for kind in range(3, 6):
            for d in range(1, side):
                piece(kind, d).start()

    g1.xevent(7)

    def take(kind):
        piece(kind, 0).wait()
        for d in range(1, side):
            piece(kind, d).wait_recv()

    def ring_rows(owner, parity):
        return pl.ds(pl.multiple_of(owner * group + parity * (group // 2), group // 2), group // 2)

    def ring(step, upward):
        owner = lax.rem(y + (-step if upward else step) + side, side)
        part = wall.at[ring_rows(owner, plane), :]
        send, recv = (r["squ"], r["rqu"]) if upward else (r["sqd"], r["rqd"])
        return remote(part, part, send.at[step], recv.at[step], sp=up if upward else down)

    def cross(t, parity):
        owner = lax.rem(y - t + side, side)
        part = wall.at[ring_rows(owner, parity), :]
        return remote(part, part, r["sqz"].at[t], r["rqz"].at[t], grp=other_plane(grp))

    def relay(step):
        if step == 0:
            @pl.when(in_plane)
            def _():
                for kind in range(3, 6):
                    piece(kind, 0).wait()

            for d in range(1, side):
                @pl.when(lax.div(lax.rem(x - d + side, side), steps) == plane)
                def _(d=d):
                    for kind in range(3, 6):
                        piece(kind, d).wait_recv()

        if step > 0:
            ring(step - 1, True).wait_recv()
        if step < steps:
            ring(step, True).start()
        cross(step, plane).start()
        if 0 < step < steps:
            ring(step - 1, False).wait_recv()
            cross(side - step, plane).start()
        if step < steps - 1:
            ring(step, False).start()

    take(0)
    take(1)
    halo1 = [
        remote(
            a.at[pl.ds(side * tok, REACH), :], a.at[pl.ds(0, REACH), :],
            r["sh1"].at[i], r["rh1"].at[i], sp=up,
        )
        for i, a in enumerate((r["ks1"], r["vs1"]))
    ]

    @pl.when(y < side - 1)
    def _():
        for copy in halo1:
            copy.start()

    g1.yevent(1, True)
    take(2)
    g1.yevent(1, False)
    relay(0)

    def between():
        g1.yevent(2, True)
        relay(1)

        @pl.when(y > 0)
        def _():
            for copy in halo1:
                copy.wait_recv()

    take_back, back1 = attend_rows(
        side, x, y, r["qs1"], r["ks1"], r["vs1"], r["band1"], r["outs1"], r["mixed1"],
        r["sb1"], r["rb1"], between,
    )
    g1.yevent(2, False)
    relay(2)
    g2.begin()
    take_back()
    g1.yevent(3, True)
    g1.yevent(3, False)
    relay(3)
    g2.xevent(1)
    g2.xevent(2)
    g2.xevent(3)
    g2.xevent(4)
    g1.yevent(4, True)
    g1.yevent(4, False)
    relay(4)
    g1.zevent()

    n = model // CUTS
    part1, theirs1 = r["part1"], r["theirs1"]
    swaps = [
        remote(
            part1.at[pl.ds(pl.multiple_of(other * half, half), half), pl.ds(i * n, n)],
            theirs1.at[:, pl.ds(i * n, n)],
            r["sp1"].at[i],
            r["rp1"].at[i],
            tp=other,
        )
        for i in range(CUTS)
    ]
    for i in range(CUTS):
        done = lax.dot_general(
            r["mixed1"][...], r["w1"][pl.ds(i * n, n), :], NT, preferred_element_type=F32
        )
        part1[:, pl.ds(i * n, n)] = done.astype(BF)
        swaps[i].start()
    g2.xevent(5)
    g2.xevent(6)
    g2.xevent(7)
    for copy in swaps:
        copy.wait_recv()

    inp, hid = r["inp"], r["hid"]
    chunk = half // 2

    def rows_of(owner, core, i):
        return pl.ds(pl.multiple_of(owner * tok + core * half + i * chunk, chunk), chunk)

    def away(step):
        return lax.rem(x + step + side, side)

    def spread(owner, send, recv, **to):
        return lambda step, i: remote(
            inp.at[rows_of(owner(step), c, i), :], inp.at[rows_of(owner(step), c, i), :],
            send.at[step, i], recv.at[step, i], **to,
        )

    pass_right = spread(lambda s: away(-s), r["sr"], r["rr"], sp=right)
    pass_left = spread(lambda s: away(s), r["sl"], r["rl"], sp=left)
    from_left = spread(lambda s: away(-s - 1), r["sr"], r["rr"], sp=right)
    from_right = spread(lambda s: away(s + 1), r["sl"], r["rl"], sp=left)

    def share(offset, i, core):
        rows = rows_of(away(offset), core, i)
        slot = offset % side
        return remote(
            inp.at[rows, :], inp.at[rows, :], r["sd"].at[slot, i], r["rd"].at[slot, i], tp=other
        )

    def show(i, core):
        rows = rows_of(0, core, i)
        return remote(hid.at[rows, :], hid.at[rows, :], r["sw"].at[i], r["rw"].at[i], tp=other)

    for i in range(2):
        rows = rows_of(0, c, i)
        sub = pl.ds(i * chunk, chunk)
        branch = part1[rows, :].astype(F32) + theirs1[sub, :].astype(F32)
        branch = branch.astype(BF).astype(F32)
        scale = lax.rsqrt(jnp.mean(branch * branch, axis=-1, keepdims=True) + EPS)
        hidden = (r["resid"][sub, :].astype(F32) + branch * scale * r["post1"][...]).astype(BF)
        hid[rows, :] = hidden
        long = hidden.astype(F32)
        scale = lax.rsqrt(jnp.mean(long * long, axis=-1, keepdims=True) + EPS)
        inp[rows_of(x, c, i), :] = (long * scale * r["pre2"][...]).astype(BF)
        pass_right(0, i).start()
        pass_left(0, i).start()
        share(0, i, c).start()
        show(i, c).start()

    shift = REACH // tok
    qs2, ks2, vs2 = r["qs2"], r["ks2"], r["vs2"]

    def halo2(owner):
        slot = owner - (side - shift)
        rows = pl.ds(pl.multiple_of(REACH + owner * tok, tok), tok)
        dest = pl.ds(pl.multiple_of(slot * tok, tok), tok)
        return [
            remote(
                a.at[rows, :], a.at[dest, :], r["sh2"].at[i, slot], r["rh2"].at[i, slot], sp=up
            )
            for i, a in enumerate((ks2, vs2))
        ]

    def qkv(offset):
        for i in range(2):
            share(offset, i, other).wait_recv()
        owner = away(offset)
        rows = pl.ds(pl.multiple_of(owner * tok, tok), tok)
        late = pl.ds(pl.multiple_of(REACH + owner * tok, tok), tok)
        done = jnp.dot(inp[rows, :], wall[...], preferred_element_type=F32).astype(BF)
        qs2[rows, :] = done[:, :head]
        ks2[late, :] = done[:, head : 2 * head]
        vs2[late, :] = done[:, 2 * head :]

        @pl.when(jnp.logical_and(owner >= side - shift, y < side - 1))
        def _():
            for copy in halo2(owner):
                copy.start()

    for t in range(side):
        cross(t, 1 - plane).wait_recv()
    qkv(0)
    last = steps - 1
    for step in range(1, steps):
        for i in range(2):
            from_left(step - 1, i).wait_recv()
            if step < last or i == 0:
                pass_right(step, i).start()
            share(-step, i, c).start()
            from_right(step - 1, i).wait_recv()
            if step < last or i == 1:
                pass_left(step, i).start()
            share(step, i, c).start()
        g2.yevent(step, True)
        qkv(-step)
        g2.yevent(step, False)
        qkv(step)
    from_left(last, 0).wait_recv()
    share(steps, 0, c).start()
    from_right(last, 1).wait_recv()
    share(steps, 1, c).start()
    qkv(steps)

    def between2():
        @pl.when(y > 0)
        def _():
            for k in range(shift):
                for copy in halo2(side - shift + k):
                    copy.wait_recv()

    take_back, back2 = attend_rows(
        side, x, y, qs2, ks2, vs2, r["band2"], r["outs2"], r["mixed2"], r["sb2"], r["rb2"],
        between2,
    )
    g2.yevent(4, True)
    g2.yevent(4, False)
    for i in range(2):
        show(i, other).wait_recv()
    take_back()
    g2.zevent()

    part2, theirs2 = r["part2"], r["theirs2"]
    swaps2 = [
        remote(
            part2.at[:, pl.ds(i * n, n)], theirs2.at[:, pl.ds(i * n, n)],
            r["sp2"].at[i], r["rp2"].at[i], tp=other,
        )
        for i in range(CUTS)
    ]
    for i in range(CUTS):
        done = lax.dot_general(
            r["mixed2"][...], r["w2"][pl.ds(i * n, n), :], NT, preferred_element_type=F32
        )
        part2[:, pl.ds(i * n, n)] = done.astype(BF)
        swaps2[i].start()
    for copy in swaps2:
        copy.wait_recv()
    for i in range(tok // chunk):
        sub = pl.ds(i * chunk, chunk)
        branch = part2[sub, :].astype(F32) + theirs2[sub, :].astype(F32)
        branch = branch.astype(BF).astype(F32)
        scale = lax.rsqrt(jnp.mean(branch * branch, axis=-1, keepdims=True) + EPS)
        done = hid[sub, :].astype(F32) + branch * scale * r["post2"][...]
        r["out"][sub, :] = done.astype(BF)

    for kind in range(3):
        for d in range(1, side):
            piece(kind, d).wait_send()

    @pl.when(in_plane)
    def _():
        for kind in range(3, 6):
            for d in range(1, side):
                piece(kind, d).wait_send()

    for step in range(steps):
        ring(step, True).wait_send()
        if step < last:
            ring(step, False).wait_send()
    for t in range(side):
        cross(t, plane).wait_send()
    g1.sent()
    g2.sent()
    back1()
    back2()
    for copy in swaps + swaps2:
        copy.wait_send()
    for step in range(steps):
        for i in range(2):
            if step < last or i == 0:
                pass_right(step, i).wait_send()
            if step < last or i == 1:
                pass_left(step, i).wait_send()
    for i in range(2):
        show(i, c).wait_send()
        for offset in range(side):
            share(offset, i, c).wait_send()

    @pl.when(y < side - 1)
    def _():
        for copy in halo1:
            copy.wait_send()
        for k in range(shift):
            for copy in halo2(side - shift + k):
                copy.wait_send()


def shards(
    side, resid, queries_first, keys_first, values_first, rel_first, post_first, out_first,
    pre_second, query_weight, key_weight, value_weight, rel_second, post_second, out_second,
):
    tok, width = queries_first.shape
    model = resid.shape[1]
    head = width // rel_first.shape[0]
    rows = side * tok
    steps = side // 2
    inputs = {
        "q": (queries_first, ANY),
        "k": (keys_first, ANY),
        "v": (values_first, ANY),
        "rel1": (rel_first, VM),
        "rel2": (rel_second, VM),
        "o1": (out_first.T, ANY),
        "o2": (out_second.T, ANY),
        "resid_any": (resid, ANY),
        "post1": (post_first[None], VM),
        "pre2": (pre_second[None], VM),
        "post2": (post_second[None], VM),
        "wq": (query_weight, ANY),
        "wk": (key_weight, ANY),
        "wv": (value_weight, ANY),
    }

    def vmem(*dims):
        return pltpu.VMEM(dims, BF)

    def dma(*dims):
        return pltpu.SemaphoreType.DMA(dims)

    scratch = {
        "wall": vmem(model, 3 * head),
        "inp": vmem(rows, model),
        "hid": vmem(tok, model),
        "resid": vmem(tok // 2, model),
        "theirs1": vmem(tok // 2, model),
        "theirs2": vmem(tok, model),
        "loads": dma(3),
        "sa2a": dma(6, side),
        "ra2a": dma(6, side),
    }
    for i in (1, 2):
        scratch[f"w{i}"] = vmem(model, width)
        scratch[f"qs{i}"] = vmem(rows, head)
        scratch[f"ks{i}"] = vmem(rows + REACH, head)
        scratch[f"vs{i}"] = vmem(rows + REACH, head)
        scratch[f"outs{i}"] = vmem(rows, head)
        scratch[f"mixed{i}"] = vmem(tok, width)
        scratch[f"part{i}"] = vmem(tok, model)
        scratch[f"band{i}"] = pltpu.VMEM((tok, tok + REACH), F32)
    for d in "sr":
        for i in (1, 2):
            scratch[f"{d}xr{i}"] = dma(steps)
            scratch[f"{d}xl{i}"] = dma(steps)
            scratch[f"{d}yu{i}"] = dma(steps, side)
            scratch[f"{d}yd{i}"] = dma(steps, side)
            scratch[f"{d}z{i}"] = dma(side, side)
            scratch[f"{d}b{i}"] = dma(side)
            scratch[f"{d}p{i}"] = dma(CUTS)
        scratch[f"{d}qu"] = dma(steps)
        scratch[f"{d}qd"] = dma(steps)
        scratch[f"{d}qz"] = dma(side)
        scratch[f"{d}h1"] = dma(2)
        scratch[f"{d}h2"] = dma(2, REACH // tok)
        scratch[f"{d}r"] = dma(steps, 2)
        scratch[f"{d}l"] = dma(steps, 2)
        scratch[f"{d}d"] = dma(side, 2)
        scratch[f"{d}w"] = dma(2)
    return pl.pallas_call(
        functools.partial(layers_kernel, side, [*inputs, "out", *scratch]),
        out_shape=jax.ShapeDtypeStruct((tok, model), BF),
        in_specs=[spec for _, spec in inputs.values()],
        out_specs=VM,
        scratch_shapes=list(scratch.values()),
        compiler_params=pltpu.CompilerParams(has_side_effects=True, collective_id=0),
    )(*(value for value, _ in inputs.values()))


def solution(mesh):
    side = math.isqrt(mesh.shape["sp"])
    in_specs = (
        P(("grp", "sp"), None),
        P(("grp", "sp"), "tp"),
        P(("grp", "sp"), "tp"),
        P(("grp", "sp"), "tp"),
        P("tp", None),
        P(),
        P("tp", "sp"),
        P(),
        P("sp", "tp"),
        P("sp", "tp"),
        P("sp", "tp"),
        P("tp", None),
        P(),
        P("tp", "sp"),
    )
    out_specs = P(("grp", "sp"), None)
    return jax.shard_map(
        functools.partial(shards, side),
        mesh=mesh,
        in_specs=in_specs,
        out_specs=out_specs,
        check_vma=False,
    )
```

time: 418 us -> 152 us (0.36)
  waiting for transfers between devices: 231 us -> 0 us
  Pallas kernels: 0 us -> 149 us
  starting transfers between devices: 84.9 us -> 0 us
  matrix products: 38.3 us -> 0 us
  local copies, waits for them, and re-layouts: 27.8 us -> 1.88 us
  blocking collectives: 16 us -> 0 us
  between operations: 14.1 us -> 0.01 us
  other arithmetic: 4.4 us -> 0 us
    pallas_call x0 -> x1, Pallas kernels: none -> 149 us  [shards(): pl.pallas_call(functools.partial(layers_kernel, side, [*inputs, 'out', *s...]
    all_gather x3 -> x0, waiting for transfers between devices: 132 us -> none  [the longest x1 113 us: in_one_piece(): lax.all_gather(both, axis, axis=dim, tiled=True)]
    ppermute x16 -> x0, waiting for transfers between devices: 98.4 us -> none  [from_behind(): lax.ppermute(value, axis, [(source, source + steps) for source in range(i...]
    ppermute x16 -> x0, starting transfers between devices: 84.8 us -> none  [from_behind(): lax.ppermute(value, axis, [(source, source + steps) for source in range(i...]
    dot_general x11 -> x0, matrix products: 33.2 us -> none  [the longest x2 9.85 us: attend_band(): jnp.einsum('nhqk,nkhd->nqhd', weights, value_band, preferred_element_type...]
    unnamed x96 -> x1, local copies, waits for them, and re-layouts: 21.1 us -> 1.88 us
    all_to_all x2 -> x0, blocking collectives: 16 us -> none  [sent_to_all(): return lax.all_to_all(copies, axis, split_axis=0, concat_axis=0, tiled=True)]
    sub x2 -> x0, matrix products: 5.07 us -> none  [attend_band(): weights = jnp.exp(scores - largest)]
  transfers between devices with their start and end apart: 19 -> 0, of which waited for: 11 -> 0; matrix products, arithmetic and copies ran while one was open for 15% -> 0% of each run, Pallas kernels for 0% -> 0%
where the time goes in v2:
time: 152 us; the launch traced here: 151 us
  Pallas kernels  149 us (98%)
  local copies, waits for them, and re-layouts  1.88 us (1%)
    pallas_call x1, Pallas kernels, shards(): pl.pallas_call(functools.partial(layers_kernel, side, [*inputs, 'out', *s...  149 us

profile of v2, /device:TPU:513, one launch (start us, length us, event | category | flops | bytes accessed | tf_op | source)
XLA Modules:
  0.0 151.3 jit_solution(15510966329929919208)
XLA Ops:
  0.0 149.4 %shard_map.136 = bf16[128,2048]{1,0:T(8,128)(2,1)} custom-call(bf16[128,1024]{1,0:T(8,128)(2,1)} %refs_0_.1, bf16[128,1024]{1,0:T(8,128)(2,1)} %refs_1_.1, bf16[128,1024]{1,0:T(8,128)(2,1)} %refs_2_.1, f32[8,257]{1,0:T(8,128)} %refs_3_.1, f32[8,257]{1,0:T(8,128)} %refs_4_.1, bf16[32,1024]{1,0:T(8,128)(2,1)} %bitcast.5, bf16[32,1024]{1,0:T(8,128)(2,1)} %bitcast.6, ...), custom_call_target="tpu_custom_call" | custom-call | tf_op jit(solution)/shard_map/pallas_call | solution.py:776
  149.4 1.9 %copy.16 = bf16[128,2048]{1,0:T(8,128)(2,1)} copy(bf16[128,2048]{1,0:T(8,128)(2,1)} %shard_map.136) | data formatting | bytes 1048576

commit v3 on v2

--- a/solution.py
+++ b/solution.py
@@ -43,7 +43,8 @@
     barrier = pltpu.get_barrier_semaphore()
     peers = [{"sp": y * side + lax.rem(x + d, side)} for d in range(1, side)]
     peers += [{"sp": lax.rem(y + d, side) * side + x} for d in (1, side - 1)]
-    peers += [{"tp": 1 - c}, {"grp": other_plane(grp)}]
+    peers += [{"tp": 1 - c}]
+    peers += [{"grp": other_plane(grp)}, {"grp": other_plane(grp), "tp": 1 - c}]
     for peer in peers:
         pl.semaphore_signal(barrier, inc=1, device_id=peer, device_id_type=MESH)
     return lambda: pl.semaphore_wait(barrier, len(peers))
@@ -132,7 +133,7 @@
 
     lax.fori_loop(0, half, early, 0)
 
-    def take_back():
+    def take_back(then):
         def finish(block, carry):
             @pl.when(block != x)
             def _():
@@ -144,6 +145,7 @@
                     rsem.at[block],
                     sp=y * side + block,
                 ).wait_recv()
+                then(block)
 
             return carry
 
@@ -170,15 +172,23 @@
 
 
 class Gather:
-    def __init__(self, side, x, y, grp, buf, xr, xl, yu, yd, z):
+    def __init__(self, side, x, y, grp, buf, shared, xr, xl, yu, yd, z):
         self.side, self.x, self.y, self.grp, self.buf = side, x, y, grp, buf
         self.xr, self.xl, self.yu, self.yd, self.z = xr, xl, yu, yd, z
+        self.shared = shared
         self.rows = buf.shape[0] // (side * side)
         quarter = buf.shape[1] // 4
-        parity = lax.rem(grp, 2)
-        self.inside = pl.ds(pl.multiple_of(parity * quarter, quarter), 3 * quarter)
-        self.across = pl.ds(pl.multiple_of(parity * 3 * quarter, quarter), quarter)
-        self.theirs = pl.ds(pl.multiple_of((1 - parity) * 3 * quarter, quarter), quarter)
+        self.plane = lax.rem(grp, 2)
+        self.inside = pl.ds(0, buf.shape[1])
+        if not shared:
+            self.inside = pl.ds(pl.multiple_of(self.plane * quarter, quarter), 3 * quarter)
+        self.across = pl.ds(pl.multiple_of(self.plane * 3 * quarter, quarter), quarter)
+        self.theirs = pl.ds(pl.multiple_of((1 - self.plane) * 3 * quarter, quarter), quarter)
+
+    def guard(self, step):
+        if self.shared:
+            return pl.when(lax.rem(self.y + step, 2) == self.plane)
+        return lambda run: run()
 
     def slab(self, xp, yp, columns):
         at = pl.multiple_of((yp * self.side + xp) * self.rows, self.rows)
@@ -224,41 +234,61 @@
         return remote(part, part, send.at[t, k], recv.at[t, k], grp=other_plane(self.grp))
 
     def begin(self):
-        self.xcopy(0, True).start()
-        self.xcopy(0, False).start()
-        self.ycopy(0, 0, True).start()
-        self.ycopy(0, 0, False).start()
+        @self.guard(0)
+        def _():
+            self.xcopy(0, True).start()
+            self.xcopy(0, False).start()
+            if self.shared:
+                self.ycopy(0, 0, True).start()
+                self.ycopy(0, 0, False).start()
 
     def xevent(self, k):
         right = k % 2 == 1
         step = (k + 1) // 2 if right else k // 2
-        self.xarrival(step - 1, right).wait_recv()
-        if step < self.side // 2 - (0 if right else 1):
-            self.xcopy(step, right).start()
-        self.ycopy(0, k, True).start()
-        self.ycopy(0, k, False).start()
-        self.zcopy(0, k, self.across).start()
-
-    def yevent(self, step, lower):
+
+        @self.guard(0)
+        def _():
+            self.xarrival(step - 1, right).wait_recv()
+            if step < self.side // 2 - (0 if right else 1):
+                self.xcopy(step, right).start()
+            if self.shared:
+                self.ycopy(0, k, True).start()
+                self.ycopy(0, k, False).start()
+            else:
+                self.zcopy(0, k, self.across).start()
+
+    def ybegin(self):
+        def one(k, carry):
+            self.ycopy(0, k, True).start()
+            self.ycopy(0, k, False).start()
+            return carry
+
+        lax.fori_loop(0, self.side, one, 0)
+
+    def yevent(self, step, base, count):
         side = self.side
         half = side // 2
         far = step == half
-        base = 0 if lower else half
+        lower = base < half
 
         def one(k, carry):
             if not far or lower:
                 self.yarrival(step - 1, k, True).wait_recv()
                 if step < half - 1 or (step == half - 1 and lower):
                     self.ycopy(step, k, True).start()
-                self.zcopy(step, k, self.across).start()
+                if not self.shared:
+                    self.zcopy(step, k, self.across).start()
             if not far or not lower:
                 self.yarrival(step - 1, k, False).wait_recv()
                 if step < half - 1 or (step == half - 1 and not lower):
                     self.ycopy(step, k, False).start()
-                self.zcopy(side - step, k, self.across).start()
+                if not self.shared:
+                    self.zcopy(side - step, k, self.across).start()
             return carry
 
-        lax.fori_loop(base, base + half, one, 0)
+        @self.guard(step)
+        def _():
+            lax.fori_loop(base, base + count, one, 0)
 
     def zevent(self):
         side = self.side
@@ -273,10 +303,15 @@
     def sent(self):
         side = self.side
         half = side // 2
+
+        @self.guard(0)
+        def _():
+            for step in range(half):
+                self.xcopy(step, True).wait_send()
+                if step < half - 1:
+                    self.xcopy(step, False).wait_send()
+
         for step in range(half):
-            self.xcopy(step, True).wait_send()
-            if step < half - 1:
-                self.xcopy(step, False).wait_send()
 
             def one(k, carry, step=step):
                 if step < half - 1:
@@ -288,13 +323,16 @@
                 self.ycopy(step, k + half, False).wait_send()
                 return carry
 
-            lax.fori_loop(0, half, one, 0)
+            @self.guard(step)
+            def _(one=one):
+                lax.fori_loop(0, half, one, 0)
 
         def one(i, carry):
             self.zcopy(lax.div(i, side), lax.rem(i, side), self.across).wait_send()
             return carry
 
-        lax.fori_loop(1, side * side, one, 0)
+        if not self.shared:
+            lax.fori_loop(1, side * side, one, 0)
 
 
 CUTS = 4
@@ -335,7 +373,7 @@
         load.start()
     g1, g2 = [
         Gather(
-            side, x, y, grp, r[f"w{i}"],
+            side, x, y, grp, r[f"w{i}"], i == 1,
             *((r[f"s{kind}{i}"], r[f"r{kind}{i}"]) for kind in ("xr", "xl", "yu", "yd", "z")),
         )
         for i in (1, 2)
@@ -382,15 +420,21 @@
         piece(1, d).start()
     g1.xevent(1)
     g1.xevent(2)
+    g1.yevent(1, 0, 2)
     for d in wide:
         piece(0, d).start()
         piece(1, d).start()
     g1.xevent(3)
     g1.xevent(4)
+    g1.yevent(1, 2, 2)
+    g1.yevent(2, 0, 2)
     for d in near:
         piece(2, d).start()
     g1.xevent(5)
     g1.xevent(6)
+    g1.yevent(1, 4, 2)
+    g1.yevent(2, 2, 2)
+    g1.yevent(3, 0, 2)
     for d in wide:
         piece(2, d).start()
 
@@ -401,6 +445,10 @@
                 piece(kind, d).start()
 
     g1.xevent(7)
+    g1.yevent(1, 6, 2)
+    g1.yevent(2, 4, 2)
+    g1.yevent(3, 2, 2)
+    g2.begin()
 
     def take(kind):
         piece(kind, 0).wait()
@@ -460,62 +508,95 @@
         for copy in halo1:
             copy.start()
 
-    g1.yevent(1, True)
     take(2)
-    g1.yevent(1, False)
+    g1.yevent(2, 6, 2)
+    g1.yevent(3, 4, 2)
     relay(0)
+    g2.xevent(1)
+    g2.xevent(2)
 
     def between():
-        g1.yevent(2, True)
+        g1.yevent(3, 6, 2)
+        g1.yevent(4, 0, 4)
         relay(1)
-
         @pl.when(y > 0)
         def _():
             for copy in halo1:
                 copy.wait_recv()
 
+
     take_back, back1 = attend_rows(
         side, x, y, r["qs1"], r["ks1"], r["vs1"], r["band1"], r["outs1"], r["mixed1"],
         r["sb1"], r["rb1"], between,
     )
-    g1.yevent(2, False)
+    g1.yevent(4, 4, 4)
     relay(2)
-    g2.begin()
-    take_back()
-    g1.yevent(3, True)
-    g1.yevent(3, False)
-    relay(3)
-    g2.xevent(1)
-    g2.xevent(2)
     g2.xevent(3)
     g2.xevent(4)
-    g1.yevent(4, True)
-    g1.yevent(4, False)
-    relay(4)
-    g1.zevent()
-
-    n = model // CUTS
-    part1, theirs1 = r["part1"], r["theirs1"]
-    swaps = [
-        remote(
-            part1.at[pl.ds(pl.multiple_of(other * half, half), half), pl.ds(i * n, n)],
-            theirs1.at[:, pl.ds(i * n, n)],
-            r["sp1"].at[i],
-            r["rp1"].at[i],
-            tp=other,
-        )
-        for i in range(CUTS)
-    ]
-    for i in range(CUTS):
-        done = lax.dot_general(
-            r["mixed1"][...], r["w1"][pl.ds(i * n, n), :], NT, preferred_element_type=F32
-        )
-        part1[:, pl.ds(i * n, n)] = done.astype(BF)
-        swaps[i].start()
+    mixed1, mixedz = r["mixed1"], r["mixedz"]
+
+    def lend(block):
+        there = pl.ds(pl.multiple_of(block * head, head), head)
+        return remote(
+            mixed1.at[:, there], mixedz.at[:, there], r["smz"].at[block], r["rmz"].at[block],
+            grp=other_plane(grp),
+        )
+
+    lend(x).start()
+    take_back(lambda block: lend(block).start())
+    relay(3)
     g2.xevent(5)
     g2.xevent(6)
+
+    n = group
+    part1, partz, terms = r["part1"], r["partz"], r["terms1"]
+    my_half = pl.ds(pl.multiple_of(c * half, half), half)
+    their_half = pl.ds(pl.multiple_of(other * half, half), half)
+
+    def columns(j):
+        return pl.ds(pl.multiple_of((2 * j + plane) * n, n), n)
+
+    swaps, same, diagonal = [], [], []
+    for j in range(steps):
+        at, lent = columns(j), (r["srz"], r["rrz"])
+        swaps.append(
+            remote(
+                part1.at[their_half, at], terms.at[1, :, at], r["sp1"].at[j], r["rp1"].at[j],
+                tp=other,
+            )
+        )
+        same.append(
+            remote(
+                partz.at[my_half, at], terms.at[0, :, at], lent[0].at[0, j], lent[1].at[0, j],
+                grp=other_plane(grp),
+            )
+        )
+        diagonal.append(
+            remote(
+                partz.at[their_half, at], terms.at[1, :, at], lent[0].at[1, j], lent[1].at[1, j],
+                grp=other_plane(grp), tp=other,
+            )
+        )
+
+    def out1(rows, j):
+        return lax.dot_general(
+            rows[...], r["w1"][columns(j), :], NT, preferred_element_type=F32
+        ).astype(BF)
+
+    for j in range(steps):
+        part1[:, columns(j)] = out1(mixed1, j)
+        swaps[j].start()
+        terms[0, :, columns(j)] = part1[my_half, columns(j)]
+    for block in range(side):
+        lend(block).wait_recv()
+    for j in range(steps):
+        partz[:, columns(j)] = out1(mixedz, j)
+        same[j].start()
+        diagonal[j].start()
+    relay(4)
     g2.xevent(7)
-    for copy in swaps:
+    g2.ybegin()
+    for copy in swaps + same + diagonal:
         copy.wait_recv()
 
     inp, hid = r["inp"], r["hid"]
@@ -552,7 +633,7 @@
     for i in range(2):
         rows = rows_of(0, c, i)
         sub = pl.ds(i * chunk, chunk)
-        branch = part1[rows, :].astype(F32) + theirs1[sub, :].astype(F32)
+        branch = terms[0, sub, :].astype(F32) + terms[1, sub, :].astype(F32)
         branch = branch.astype(BF).astype(F32)
         scale = lax.rsqrt(jnp.mean(branch * branch, axis=-1, keepdims=True) + EPS)
         hidden = (r["resid"][sub, :].astype(F32) + branch * scale * r["post1"][...]).astype(BF)
@@ -609,9 +690,9 @@
             if step < last or i == 1:
                 pass_left(step, i).start()
             share(step, i, c).start()
-        g2.yevent(step, True)
+        g2.yevent(step, 0, 4)
         qkv(-step)
-        g2.yevent(step, False)
+        g2.yevent(step, 4, 4)
         qkv(step)
     from_left(last, 0).wait_recv()
     share(steps, 0, c).start()
@@ -630,14 +711,15 @@
         side, x, y, qs2, ks2, vs2, r["band2"], r["outs2"], r["mixed2"], r["sb2"], r["rb2"],
         between2,
     )
-    g2.yevent(4, True)
-    g2.yevent(4, False)
+    g2.yevent(4, 0, 4)
+    g2.yevent(4, 4, 4)
     for i in range(2):
         show(i, other).wait_recv()
-    take_back()
+    take_back(lambda block: None)
     g2.zevent()
 
     part2, theirs2 = r["part2"], r["theirs2"]
+    n = model // CUTS
     swaps2 = [
         remote(
             part2.at[:, pl.ds(i * n, n)], theirs2.at[:, pl.ds(i * n, n)],
@@ -681,8 +763,10 @@
     g2.sent()
     back1()
     back2()
-    for copy in swaps + swaps2:
+    for copy in swaps + same + diagonal + swaps2:
         copy.wait_send()
+    for block in range(side):
+        lend(block).wait_send()
     for step in range(steps):
         for i in range(2):
             if step < last or i == 0:
@@ -740,7 +824,9 @@
         "inp": vmem(rows, model),
         "hid": vmem(tok, model),
         "resid": vmem(tok // 2, model),
-        "theirs1": vmem(tok // 2, model),
+        "terms1": vmem(2, tok // 2, model),
+        "mixedz": vmem(tok, width),
+        "partz": vmem(tok, model),
         "theirs2": vmem(tok, model),
         "loads": dma(3),
         "sa2a": dma(6, side),
@@ -764,6 +850,8 @@
             scratch[f"{d}z{i}"] = dma(side, side)
             scratch[f"{d}b{i}"] = dma(side)
             scratch[f"{d}p{i}"] = dma(CUTS)
+        scratch[f"{d}mz"] = dma(side)
+        scratch[f"{d}rz"] = dma(2, steps)
         scratch[f"{d}qu"] = dma(steps)
         scratch[f"{d}qd"] = dma(steps)
         scratch[f"{d}qz"] = dma(side)

time: 152 us -> 149 us (0.980)
  Pallas kernels: 149 us -> 145 us
    pallas_call x1, Pallas kernels: 149 us -> 145 us  [shards(): pl.pallas_call(functools.partial(layers_kernel, side, [*inputs, 'out', *s...]
where the time goes in v3:
time: 149 us; the launch traced here: 147 us
  Pallas kernels  145 us (97%)
  local copies, waits for them, and re-layouts  1.88 us (1%)
    pallas_call x1, Pallas kernels, shards(): pl.pallas_call(functools.partial(layers_kernel, side, [*inputs, 'out', *s...  145 us

profile of v3, /device:TPU:513, one launch (start us, length us, event | category | flops | bytes accessed | tf_op | source)
XLA Modules:
  0.0 146.8 jit_solution(10110015609089217939)
XLA Ops:
  0.0 144.9 %shard_map.136 = bf16[128,2048]{1,0:T(8,128)(2,1)} custom-call(bf16[128,1024]{1,0:T(8,128)(2,1)} %refs_0_.1, bf16[128,1024]{1,0:T(8,128)(2,1)} %refs_1_.1, bf16[128,1024]{1,0:T(8,128)(2,1)} %refs_2_.1, f32[8,257]{1,0:T(8,128)} %refs_3_.1, f32[8,257]{1,0:T(8,128)} %refs_4_.1, bf16[32,1024]{1,0:T(8,128)(2,1)} %bitcast.5, bf16[32,1024]{1,0:T(8,128)(2,1)} %bitcast.6, ...), custom_call_target="tpu_custom_call" | custom-call | tf_op jit(solution)/shard_map/pallas_call | solution.py:864
  144.9 1.9 %copy.16 = bf16[128,2048]{1,0:T(8,128)(2,1)} copy(bf16[128,2048]{1,0:T(8,128)(2,1)} %shard_map.136) | data formatting | bytes 1048576

commit v4 on v3

--- a/solution.py
+++ b/solution.py
@@ -257,13 +257,10 @@
             else:
                 self.zcopy(0, k, self.across).start()
 
-    def ybegin(self):
-        def one(k, carry):
+    def ybegin(self, *pieces):
+        for k in pieces:
             self.ycopy(0, k, True).start()
             self.ycopy(0, k, False).start()
-            return carry
-
-        lax.fori_loop(0, self.side, one, 0)
 
     def yevent(self, step, base, count):
         side = self.side
@@ -413,43 +410,6 @@
         load.wait()
     meet()
 
-    g1.begin()
-    near, wide = [1, side - 1, 2, side - 2], [3, side - 3, 4]
-    for d in near:
-        piece(0, d).start()
-        piece(1, d).start()
-    g1.xevent(1)
-    g1.xevent(2)
-    g1.yevent(1, 0, 2)
-    for d in wide:
-        piece(0, d).start()
-        piece(1, d).start()
-    g1.xevent(3)
-    g1.xevent(4)
-    g1.yevent(1, 2, 2)
-    g1.yevent(2, 0, 2)
-    for d in near:
-        piece(2, d).start()
-    g1.xevent(5)
-    g1.xevent(6)
-    g1.yevent(1, 4, 2)
-    g1.yevent(2, 2, 2)
-    g1.yevent(3, 0, 2)
-    for d in wide:
-        piece(2, d).start()
-
-    @pl.when(in_plane)
-    def _():
-        for kind in range(3, 6):
-            for d in range(1, side):
-                piece(kind, d).start()
-
-    g1.xevent(7)
-    g1.yevent(1, 6, 2)
-    g1.yevent(2, 4, 2)
-    g1.yevent(3, 2, 2)
-    g2.begin()
-
     def take(kind):
         piece(kind, 0).wait()
         for d in range(1, side):
@@ -486,13 +446,88 @@
             ring(step - 1, True).wait_recv()
         if step < steps:
             ring(step, True).start()
-        cross(step, plane).start()
+        if step > 0:
+            cross(step, plane).start()
         if 0 < step < steps:
             ring(step - 1, False).wait_recv()
+        if 0 < step < steps:
             cross(side - step, plane).start()
         if step < steps - 1:
             ring(step, False).start()
 
+    g1.begin()
+
+    opposite = side // 2
+    odd = lax.rem(x, 2) == 1
+    far_x = lax.rem(x + opposite, side)
+    far_cut = pl.ds(pl.multiple_of(far_x * head, head), head)
+    behind = pl.ds(pl.multiple_of(REACH + lax.rem(x + 1, side) * tok, tok), tok)
+    behind_q = pl.ds(pl.multiple_of(lax.rem(x + 1, side) * tok, tok), tok)
+
+    def detour(kind):
+        src = v_ref if kind == 1 else q_ref
+        return remote(
+            src.at[:, far_cut], r["via"].at[kind - 1], r["sv"].at[kind, 0], r["rv"].at[kind - 1],
+            sp=left,
+        )
+
+    def onward(kind):
+        dst = r["vs1"].at[behind, :] if kind == 1 else r["qs1"].at[behind_q, :]
+        return remote(
+            r["via"].at[kind - 1], dst, r["sv"].at[kind, 1], r["ra2a"].at[kind, opposite],
+            sp=y * side + lax.rem(x + opposite + 1, side),
+        )
+
+    def hand_out(kinds, distances):
+        for d in distances:
+            for kind in kinds:
+                piece(kind, d).start()
+
+    near, third = [1, side - 1, 2, side - 2], [3, side - 3]
+    hand_out([0], near)
+    g1.xevent(1)
+    g1.xevent(2)
+    hand_out([1], near)
+    detour(1).start()
+    g1.xevent(3)
+    g1.xevent(4)
+    hand_out([0], third + [opposite])
+    g1.yevent(1, 0, 2)
+    g1.xevent(5)
+    g1.xevent(6)
+    hand_out([1], third)
+    detour(1).wait_recv()
+    onward(1).start()
+
+    @pl.when(odd)
+    def _():
+        detour(2).start()
+
+    g1.yevent(1, 2, 2)
+    g1.yevent(2, 0, 2)
+    g1.xevent(7)
+
+    @pl.when(jnp.logical_not(odd))
+    def _():
+        hand_out([2], [opposite])
+
+    hand_out([2], third + near)
+
+    @pl.when(in_plane)
+    def _():
+        hand_out([3, 4, 5], range(1, side))
+
+    @pl.when(jnp.logical_not(odd))
+    def _():
+        detour(2).wait_recv()
+        onward(2).start()
+
+    g1.yevent(1, 4, 2)
+    g1.yevent(2, 2, 2)
+    g1.yevent(3, 0, 2)
+    g1.yevent(1, 6, 2)
+    g1.yevent(2, 4, 2)
+    g1.yevent(3, 2, 2)
     take(0)
     take(1)
     halo1 = [
@@ -509,16 +544,11 @@
             copy.start()
 
     take(2)
-    g1.yevent(2, 6, 2)
-    g1.yevent(3, 4, 2)
-    relay(0)
-    g2.xevent(1)
-    g2.xevent(2)
+    g2.begin()
 
     def between():
-        g1.yevent(3, 6, 2)
-        g1.yevent(4, 0, 4)
-        relay(1)
+        g1.yevent(2, 6, 2)
+        g1.yevent(3, 4, 2)
         @pl.when(y > 0)
         def _():
             for copy in halo1:
@@ -529,10 +559,12 @@
         side, x, y, r["qs1"], r["ks1"], r["vs1"], r["band1"], r["outs1"], r["mixed1"],
         r["sb1"], r["rb1"], between,
     )
+    g1.yevent(3, 6, 2)
+    relay(0)
+    g2.xevent(1)
+    g2.xevent(2)
+    g1.yevent(4, 0, 4)
     g1.yevent(4, 4, 4)
-    relay(2)
-    g2.xevent(3)
-    g2.xevent(4)
     mixed1, mixedz = r["mixed1"], r["mixedz"]
 
     def lend(block):
@@ -544,9 +576,6 @@
 
     lend(x).start()
     take_back(lambda block: lend(block).start())
-    relay(3)
-    g2.xevent(5)
-    g2.xevent(6)
 
     n = group
     part1, partz, terms = r["part1"], r["partz"], r["terms1"]
@@ -587,15 +616,17 @@
         part1[:, columns(j)] = out1(mixed1, j)
         swaps[j].start()
         terms[0, :, columns(j)] = part1[my_half, columns(j)]
+    g2.xevent(3)
+    g2.xevent(4)
     for block in range(side):
         lend(block).wait_recv()
     for j in range(steps):
         partz[:, columns(j)] = out1(mixedz, j)
         same[j].start()
         diagonal[j].start()
-    relay(4)
-    g2.xevent(7)
-    g2.ybegin()
+    cross(0, plane).start()
+    relay(1)
+    g2.ybegin(0, 1, 2)
     for copy in swaps + same + diagonal:
         copy.wait_recv()
 
@@ -676,10 +707,27 @@
             for copy in halo2(owner):
                 copy.start()
 
-    for t in range(side):
-        cross(t, 1 - plane).wait_recv()
-    qkv(0)
+    relay(2)
+    g2.ybegin(3, 4)
+    g2.xevent(5)
+    g2.xevent(6)
     last = steps - 1
+
+    def fill(step, i):
+        if (step, i) == (1, 0):
+            relay(3)
+            g2.ybegin(5, 6)
+        elif (step, i) == (1, 1):
+            relay(4)
+            g2.xevent(7)
+            g2.ybegin(7)
+        elif (step, i) == (2, 0):
+            g2.yevent(1, 0, 4)
+        elif (step, i) == (2, 1):
+            g2.yevent(1, 4, 4)
+        elif (step, i) == (3, 0):
+            g2.yevent(2, 0, 4)
+
     for step in range(1, steps):
         for i in range(2):
             from_left(step - 1, i).wait_recv()
@@ -690,15 +738,21 @@
             if step < last or i == 1:
                 pass_left(step, i).start()
             share(step, i, c).start()
-        g2.yevent(step, 0, 4)
-        qkv(-step)
-        g2.yevent(step, 4, 4)
-        qkv(step)
+            fill(step, i)
+    for t in range(side):
+        cross(t, 1 - plane).wait_recv()
+    qkv(0)
+    for d in range(1, steps):
+        qkv(-d)
+        qkv(d)
+    g2.yevent(2, 4, 4)
     from_left(last, 0).wait_recv()
     share(steps, 0, c).start()
     from_right(last, 1).wait_recv()
     share(steps, 1, c).start()
     qkv(steps)
+
+    g2.yevent(3, 0, 4)
 
     def between2():
         @pl.when(y > 0)
@@ -707,15 +761,17 @@
                 for copy in halo2(side - shift + k):
                     copy.wait_recv()
 
+        g2.yevent(3, 4, 4)
+
     take_back, back2 = attend_rows(
         side, x, y, qs2, ks2, vs2, r["band2"], r["outs2"], r["mixed2"], r["sb2"], r["rb2"],
         between2,
     )
     g2.yevent(4, 0, 4)
-    g2.yevent(4, 4, 4)
     for i in range(2):
         show(i, other).wait_recv()
     take_back(lambda block: None)
+    g2.yevent(4, 4, 4)
     g2.zevent()
 
     part2, theirs2 = r["part2"], r["theirs2"]
@@ -745,7 +801,19 @@
 
     for kind in range(3):
         for d in range(1, side):
-            piece(kind, d).wait_send()
+            if kind == 0 or d != opposite:
+                piece(kind, d).wait_send()
+    detour(1).wait_send()
+    onward(1).wait_send()
+
+    @pl.when(odd)
+    def _():
+        detour(2).wait_send()
+
+    @pl.when(jnp.logical_not(odd))
+    def _():
+        onward(2).wait_send()
+        piece(2, opposite).wait_send()
 
     @pl.when(in_plane)
     def _():
@@ -829,6 +897,9 @@
         "partz": vmem(tok, model),
         "theirs2": vmem(tok, model),
         "loads": dma(3),
+        "via": vmem(2, tok, head),
+        "sv": dma(3, 2),
+        "rv": dma(2),
         "sa2a": dma(6, side),
         "ra2a": dma(6, side),
     }

time: 149 us -> 142 us (0.953)
  Pallas kernels: 145 us -> 139 us
    pallas_call x1, Pallas kernels: 145 us -> 139 us  [shards(): pl.pallas_call(functools.partial(layers_kernel, side, [*inputs, 'out', *s...]
where the time goes in v4:
time: 142 us; the launch traced here: 141 us
  Pallas kernels  139 us (98%)
  local copies, waits for them, and re-layouts  1.88 us (1%)
    pallas_call x1, Pallas kernels, shards(): pl.pallas_call(functools.partial(layers_kernel, side, [*inputs, 'out', *s...  139 us

profile of v4, /device:TPU:513, one launch (start us, length us, event | category | flops | bytes accessed | tf_op | source)
XLA Modules:
  0.0 141.0 jit_solution(9926074726534610989)
XLA Ops:
  0.0 139.1 %shard_map.136 = bf16[128,2048]{1,0:T(8,128)(2,1)} custom-call(bf16[128,1024]{1,0:T(8,128)(2,1)} %refs_0_.1, bf16[128,1024]{1,0:T(8,128)(2,1)} %refs_1_.1, bf16[128,1024]{1,0:T(8,128)(2,1)} %refs_2_.1, f32[8,257]{1,0:T(8,128)} %refs_3_.1, f32[8,257]{1,0:T(8,128)} %refs_4_.1, bf16[32,1024]{1,0:T(8,128)(2,1)} %bitcast.5, bf16[32,1024]{1,0:T(8,128)(2,1)} %bitcast.6, ...), custom_call_target="tpu_custom_call" | custom-call | tf_op jit(solution)/shard_map/pallas_call | solution.py:935
  139.1 1.9 %copy.16 = bf16[128,2048]{1,0:T(8,128)(2,1)} copy(bf16[128,2048]{1,0:T(8,128)(2,1)} %shard_map.136) | data formatting | bytes 1048576

commit v5 on v4

--- a/solution.py
+++ b/solution.py
@@ -503,24 +503,26 @@
     def _():
         detour(2).start()
 
+    @pl.when(jnp.logical_not(odd))
+    def _():
+        hand_out([2], [opposite])
+
+    hand_out([2], third + near)
+
+    @pl.when(in_plane)
+    def _():
+        hand_out([3, 4, 5], range(1, side))
+
     g1.yevent(1, 2, 2)
     g1.yevent(2, 0, 2)
     g1.xevent(7)
 
     @pl.when(jnp.logical_not(odd))
     def _():
-        hand_out([2], [opposite])
-
-    hand_out([2], third + near)
-
-    @pl.when(in_plane)
-    def _():
-        hand_out([3, 4, 5], range(1, side))
-
-    @pl.when(jnp.logical_not(odd))
-    def _():
         detour(2).wait_recv()
         onward(2).start()
+
+    g2.begin()
 
     g1.yevent(1, 4, 2)
     g1.yevent(2, 2, 2)
@@ -544,11 +546,12 @@
             copy.start()
 
     take(2)
-    g2.begin()
 
     def between():
         g1.yevent(2, 6, 2)
         g1.yevent(3, 4, 2)
+        g2.xevent(1)
+        g2.xevent(2)
         @pl.when(y > 0)
         def _():
             for copy in halo1:
@@ -561,8 +564,8 @@
     )
     g1.yevent(3, 6, 2)
     relay(0)
-    g2.xevent(1)
-    g2.xevent(2)
+    g2.xevent(3)
+    g2.xevent(4)
     g1.yevent(4, 0, 4)
     g1.yevent(4, 4, 4)
     mixed1, mixedz = r["mixed1"], r["mixedz"]
@@ -616,8 +619,8 @@
         part1[:, columns(j)] = out1(mixed1, j)
         swaps[j].start()
         terms[0, :, columns(j)] = part1[my_half, columns(j)]
-    g2.xevent(3)
-    g2.xevent(4)
+    g2.xevent(5)
+    g2.xevent(6)
     for block in range(side):
         lend(block).wait_recv()
     for j in range(steps):
@@ -626,7 +629,7 @@
         diagonal[j].start()
     cross(0, plane).start()
     relay(1)
-    g2.ybegin(0, 1, 2)
+    g2.ybegin(0, 1, 2, 3)
     for copy in swaps + same + diagonal:
         copy.wait_recv()
 
@@ -708,24 +711,28 @@
                 copy.start()
 
     relay(2)
-    g2.ybegin(3, 4)
-    g2.xevent(5)
-    g2.xevent(6)
+    g2.ybegin(4, 5, 6)
+    g2.xevent(7)
     last = steps - 1
 
     def fill(step, i):
         if (step, i) == (1, 0):
             relay(3)
-            g2.ybegin(5, 6)
+            g2.ybegin(7)
         elif (step, i) == (1, 1):
             relay(4)
-            g2.xevent(7)
-            g2.ybegin(7)
         elif (step, i) == (2, 0):
             g2.yevent(1, 0, 4)
         elif (step, i) == (2, 1):
             g2.yevent(1, 4, 4)
+            for t in range(side):
+                cross(t, 1 - plane).wait_recv()
+            qkv(0)
+            qkv(-1)
+            qkv(1)
         elif (step, i) == (3, 0):
+            qkv(-2)
+            qkv(2)
             g2.yevent(2, 0, 4)
 
     for step in range(1, steps):
@@ -739,20 +746,15 @@
                 pass_left(step, i).start()
             share(step, i, c).start()
             fill(step, i)
-    for t in range(side):
-        cross(t, 1 - plane).wait_recv()
-    qkv(0)
-    for d in range(1, steps):
-        qkv(-d)
-        qkv(d)
-    g2.yevent(2, 4, 4)
+    qkv(-last)
+    qkv(last)
     from_left(last, 0).wait_recv()
     share(steps, 0, c).start()
     from_right(last, 1).wait_recv()
     share(steps, 1, c).start()
     qkv(steps)
 
-    g2.yevent(3, 0, 4)
+    g2.yevent(2, 4, 4)
 
     def between2():
         @pl.when(y > 0)
@@ -761,44 +763,18 @@
                 for copy in halo2(side - shift + k):
                     copy.wait_recv()
 
-        g2.yevent(3, 4, 4)
+        g2.yevent(3, 0, 4)
 
     take_back, back2 = attend_rows(
         side, x, y, qs2, ks2, vs2, r["band2"], r["outs2"], r["mixed2"], r["sb2"], r["rb2"],
         between2,
     )
+    g2.yevent(3, 4, 4)
     g2.yevent(4, 0, 4)
     for i in range(2):
         show(i, other).wait_recv()
     take_back(lambda block: None)
     g2.yevent(4, 4, 4)
-    g2.zevent()
-
-    part2, theirs2 = r["part2"], r["theirs2"]
-    n = model // CUTS
-    swaps2 = [
-        remote(
-            part2.at[:, pl.ds(i * n, n)], theirs2.at[:, pl.ds(i * n, n)],
-            r["sp2"].at[i], r["rp2"].at[i], tp=other,
-        )
-        for i in range(CUTS)
-    ]
-    for i in range(CUTS):
-        done = lax.dot_general(
-            r["mixed2"][...], r["w2"][pl.ds(i * n, n), :], NT, preferred_element_type=F32
-        )
-        part2[:, pl.ds(i * n, n)] = done.astype(BF)
-        swaps2[i].start()
-    for copy in swaps2:
-        copy.wait_recv()
-    for i in range(tok // chunk):
-        sub = pl.ds(i * chunk, chunk)
-        branch = part2[sub, :].astype(F32) + theirs2[sub, :].astype(F32)
-        branch = branch.astype(BF).astype(F32)
-        scale = lax.rsqrt(jnp.mean(branch * branch, axis=-1, keepdims=True) + EPS)
-        done = hid[sub, :].astype(F32) + branch * scale * r["post2"][...]
-        r["out"][sub, :] = done.astype(BF)
-
     for kind in range(3):
         for d in range(1, side):
             if kind == 0 or d != opposite:
@@ -828,10 +804,8 @@
     for t in range(side):
         cross(t, plane).wait_send()
     g1.sent()
-    g2.sent()
     back1()
-    back2()
-    for copy in swaps + same + diagonal + swaps2:
+    for copy in swaps + same + diagonal:
         copy.wait_send()
     for block in range(side):
         lend(block).wait_send()
@@ -853,6 +827,38 @@
         for k in range(shift):
             for copy in halo2(side - shift + k):
                 copy.wait_send()
+
+    g2.sent()
+    back2()
+    g2.zevent()
+
+    part2, theirs2 = r["part2"], r["theirs2"]
+    n = model // CUTS
+    swaps2 = [
+        remote(
+            part2.at[:, pl.ds(i * n, n)], theirs2.at[:, pl.ds(i * n, n)],
+            r["sp2"].at[i], r["rp2"].at[i], tp=other,
+        )
+        for i in range(CUTS)
+    ]
+    for i in range(CUTS):
+        done = lax.dot_general(
+            r["mixed2"][...], r["w2"][pl.ds(i * n, n), :], NT, preferred_element_type=F32
+        )
+        part2[:, pl.ds(i * n, n)] = done.astype(BF)
+        swaps2[i].start()
+    for copy in swaps2:
+        copy.wait_recv()
+    for i in range(tok // chunk):
+        sub = pl.ds(i * chunk, chunk)
+        branch = part2[sub, :].astype(F32) + theirs2[sub, :].astype(F32)
+        branch = branch.astype(BF).astype(F32)
+        scale = lax.rsqrt(jnp.mean(branch * branch, axis=-1, keepdims=True) + EPS)
+        done = hid[sub, :].astype(F32) + branch * scale * r["post2"][...]
+        r["out"][sub, :] = done.astype(BF)
+
+    for copy in swaps2:
+        copy.wait_send()
 
 
 def shards(

time: 142 us -> 138 us (0.972)
  Pallas kernels: 139 us -> 136 us
    pallas_call x1, Pallas kernels: 139 us -> 136 us  [shards(): pl.pallas_call(functools.partial(layers_kernel, side, [*inputs, 'out', *s...]
where the time goes in v5:
time: 138 us
  Pallas kernels  136 us (99%)
  local copies, waits for them, and re-layouts  1.88 us (1%)
    pallas_call x1, Pallas kernels, shards(): pl.pallas_call(functools.partial(layers_kernel, side, [*inputs, 'out', *s...  136 us

profile of v5, /device:TPU:513, one launch (start us, length us, event | category | flops | bytes accessed | tf_op | source)
XLA Modules:
  0.0 137.6 jit_solution(16837745846426711416)
XLA Ops:
  0.0 135.7 %shard_map.136 = bf16[128,2048]{1,0:T(8,128)(2,1)} custom-call(bf16[128,1024]{1,0:T(8,128)(2,1)} %refs_0_.1, bf16[128,1024]{1,0:T(8,128)(2,1)} %refs_1_.1, bf16[128,1024]{1,0:T(8,128)(2,1)} %refs_2_.1, f32[8,257]{1,0:T(8,128)} %refs_3_.1, f32[8,257]{1,0:T(8,128)} %refs_4_.1, bf16[32,1024]{1,0:T(8,128)(2,1)} %bitcast.5, bf16[32,1024]{1,0:T(8,128)(2,1)} %bitcast.6, ...), custom_call_target="tpu_custom_call" | custom-call | tf_op jit(solution)/shard_map/pallas_call | solution.py:941
  135.7 1.9 %copy.16 = bf16[128,2048]{1,0:T(8,128)(2,1)} copy(bf16[128,2048]{1,0:T(8,128)(2,1)} %shard_map.136) | data formatting | bytes 1048576

commit v6 on v5

--- a/solution.py
+++ b/solution.py
@@ -44,7 +44,7 @@
     peers = [{"sp": y * side + lax.rem(x + d, side)} for d in range(1, side)]
     peers += [{"sp": lax.rem(y + d, side) * side + x} for d in (1, side - 1)]
     peers += [{"tp": 1 - c}]
-    peers += [{"grp": other_plane(grp)}, {"grp": other_plane(grp), "tp": 1 - c}]
+    peers += [{"grp": other_plane(grp)}]
     for peer in peers:
         pl.semaphore_signal(barrier, inc=1, device_id=peer, device_id_type=MESH)
     return lambda: pl.semaphore_wait(barrier, len(peers))
@@ -446,11 +446,11 @@
             ring(step - 1, True).wait_recv()
         if step < steps:
             ring(step, True).start()
-        if step > 0:
+        if step > 1:
             cross(step, plane).start()
         if 0 < step < steps:
             ring(step - 1, False).wait_recv()
-        if 0 < step < steps:
+        if 1 < step < steps:
             cross(side - step, plane).start()
         if step < steps - 1:
             ring(step, False).start()
@@ -588,7 +588,7 @@
     def columns(j):
         return pl.ds(pl.multiple_of((2 * j + plane) * n, n), n)
 
-    swaps, same, diagonal = [], [], []
+    swaps, pooled, given = [], [], []
     for j in range(steps):
         at, lent = columns(j), (r["srz"], r["rrz"])
         swaps.append(
@@ -597,16 +597,16 @@
                 tp=other,
             )
         )
-        same.append(
+        pooled.append(
             remote(
-                partz.at[my_half, at], terms.at[0, :, at], lent[0].at[0, j], lent[1].at[0, j],
+                partz.at[their_half, at], r["pool"].at[:, at], lent[0].at[0, j], lent[1].at[0, j],
+                tp=other,
+            )
+        )
+        given.append(
+            remote(
+                r["sums"].at[:, at], terms.at[0, :, at], lent[0].at[1, j], lent[1].at[1, j],
                 grp=other_plane(grp),
-            )
-        )
-        diagonal.append(
-            remote(
-                partz.at[their_half, at], terms.at[1, :, at], lent[0].at[1, j], lent[1].at[1, j],
-                grp=other_plane(grp), tp=other,
             )
         )
 
@@ -619,18 +619,29 @@
         part1[:, columns(j)] = out1(mixed1, j)
         swaps[j].start()
         terms[0, :, columns(j)] = part1[my_half, columns(j)]
+        rest = pl.ds(pl.multiple_of((2 * j + 1 - plane) * n, n), n)
+        terms[1, :, rest] = jnp.zeros((half, n), BF)
     g2.xevent(5)
     g2.xevent(6)
+    relay(1)
+    g2.ybegin(0, 1, 2, 3)
     for block in range(side):
         lend(block).wait_recv()
-    for j in range(steps):
-        partz[:, columns(j)] = out1(mixedz, j)
-        same[j].start()
-        diagonal[j].start()
-    cross(0, plane).start()
-    relay(1)
-    g2.ybegin(0, 1, 2, 3)
-    for copy in swaps + same + diagonal:
+    for j in range(steps + 2):
+        if j < steps:
+            partz[:, columns(j)] = out1(mixedz, j)
+            pooled[j].start()
+        if j >= 2:
+            at = columns(j - 2)
+            pooled[j - 2].wait_recv()
+            both = partz[my_half, at].astype(F32) + r["pool"][:, at].astype(F32)
+            r["sums"][:, at] = both.astype(BF)
+            given[j - 2].start()
+    for t in (0, 1, side - 1):
+        cross(t, plane).start()
+    relay(2)
+    g2.ybegin(4, 5, 6)
+    for copy in swaps + given:
         copy.wait_recv()
 
     inp, hid = r["inp"], r["hid"]
@@ -710,30 +721,29 @@
             for copy in halo2(owner):
                 copy.start()
 
-    relay(2)
-    g2.ybegin(4, 5, 6)
+    relay(3)
     g2.xevent(7)
+    g2.ybegin(7)
     last = steps - 1
 
     def fill(step, i):
         if (step, i) == (1, 0):
-            relay(3)
-            g2.ybegin(7)
+            relay(4)
         elif (step, i) == (1, 1):
-            relay(4)
+            g2.yevent(1, 0, 4)
         elif (step, i) == (2, 0):
-            g2.yevent(1, 0, 4)
+            g2.yevent(1, 4, 4)
         elif (step, i) == (2, 1):
-            g2.yevent(1, 4, 4)
             for t in range(side):
                 cross(t, 1 - plane).wait_recv()
             qkv(0)
             qkv(-1)
             qkv(1)
+            g2.yevent(2, 0, 4)
         elif (step, i) == (3, 0):
             qkv(-2)
             qkv(2)
-            g2.yevent(2, 0, 4)
+            g2.yevent(2, 4, 4)
 
     for step in range(1, steps):
         for i in range(2):
@@ -754,7 +764,7 @@
     share(steps, 1, c).start()
     qkv(steps)
 
-    g2.yevent(2, 4, 4)
+    g2.yevent(3, 0, 4)
 
     def between2():
         @pl.when(y > 0)
@@ -763,13 +773,12 @@
                 for copy in halo2(side - shift + k):
                     copy.wait_recv()
 
-        g2.yevent(3, 0, 4)
+        g2.yevent(3, 4, 4)
 
     take_back, back2 = attend_rows(
         side, x, y, qs2, ks2, vs2, r["band2"], r["outs2"], r["mixed2"], r["sb2"], r["rb2"],
         between2,
     )
-    g2.yevent(3, 4, 4)
     g2.yevent(4, 0, 4)
     for i in range(2):
         show(i, other).wait_recv()
@@ -805,7 +814,7 @@
         cross(t, plane).wait_send()
     g1.sent()
     back1()
-    for copy in swaps + same + diagonal:
+    for copy in swaps + pooled + given:
         copy.wait_send()
     for block in range(side):
         lend(block).wait_send()
@@ -901,6 +910,8 @@
         "terms1": vmem(2, tok // 2, model),
         "mixedz": vmem(tok, width),
         "partz": vmem(tok, model),
+        "pool": vmem(tok // 2, model),
+        "sums": vmem(tok // 2, model),
         "theirs2": vmem(tok, model),
         "loads": dma(3),
         "via": vmem(2, tok, head),

time: 138 us -> 136 us (0.986)
  Pallas kernels: 136 us -> 134 us
    pallas_call x1, Pallas kernels: 136 us -> 134 us  [shards(): pl.pallas_call(functools.partial(layers_kernel, side, [*inputs, 'out', *s...]
where the time goes in v6:
time: 136 us
  Pallas kernels  134 us (99%)
  local copies, waits for them, and re-layouts  1.88 us (1%)
    pallas_call x1, Pallas kernels, shards(): pl.pallas_call(functools.partial(layers_kernel, side, [*inputs, 'out', *s...  134 us

profile of v6, /device:TPU:513, one launch (start us, length us, event | category | flops | bytes accessed | tf_op | source)
XLA Modules:
  0.0 135.7 jit_solution(5738944106171977590)
XLA Ops:
  0.0 133.8 %shard_map.136 = bf16[128,2048]{1,0:T(8,128)(2,1)} custom-call(bf16[128,1024]{1,0:T(8,128)(2,1)} %refs_0_.1, bf16[128,1024]{1,0:T(8,128)(2,1)} %refs_1_.1, bf16[128,1024]{1,0:T(8,128)(2,1)} %refs_2_.1, f32[8,257]{1,0:T(8,128)} %refs_3_.1, f32[8,257]{1,0:T(8,128)} %refs_4_.1, bf16[32,1024]{1,0:T(8,128)(2,1)} %bitcast.5, bf16[32,1024]{1,0:T(8,128)(2,1)} %bitcast.6, ...), custom_call_target="tpu_custom_call" | custom-call | tf_op jit(solution)/shard_map/pallas_call | solution.py:952
  133.8 1.9 %copy.16 = bf16[128,2048]{1,0:T(8,128)(2,1)} copy(bf16[128,2048]{1,0:T(8,128)(2,1)} %shard_map.136) | data formatting | bytes 1048576

commit v7 on v6

--- a/solution.py
+++ b/solution.py
@@ -780,9 +780,6 @@
         between2,
     )
     g2.yevent(4, 0, 4)
-    for i in range(2):
-        show(i, other).wait_recv()
-    take_back(lambda block: None)
     g2.yevent(4, 4, 4)
     for kind in range(3):
         for d in range(1, side):
@@ -828,17 +825,9 @@
         show(i, c).wait_send()
         for offset in range(side):
             share(offset, i, c).wait_send()
-
-    @pl.when(y < side - 1)
-    def _():
-        for copy in halo1:
-            copy.wait_send()
-        for k in range(shift):
-            for copy in halo2(side - shift + k):
-                copy.wait_send()
-
-    g2.sent()
-    back2()
+    for i in range(2):
+        show(i, other).wait_recv()
+    take_back(lambda block: None)
     g2.zevent()
 
     part2, theirs2 = r["part2"], r["theirs2"]
@@ -856,6 +845,16 @@
         )
         part2[:, pl.ds(i * n, n)] = done.astype(BF)
         swaps2[i].start()
+    @pl.when(y < side - 1)
+    def _():
+        for copy in halo1:
+            copy.wait_send()
+        for k in range(shift):
+            for copy in halo2(side - shift + k):
+                copy.wait_send()
+
+    g2.sent()
+    back2()
     for copy in swaps2:
         copy.wait_recv()
     for i in range(tok // chunk):

time: 136 us -> 134 us (0.985); the launches traced: 136 us -> 132 us
  Pallas kernels: 134 us -> 130 us
    pallas_call x1, Pallas kernels: 134 us -> 130 us  [shards(): pl.pallas_call(functools.partial(layers_kernel, side, [*inputs, 'out', *s...]
where the time goes in v7:
time: 134 us; the launch traced here: 132 us
  Pallas kernels  130 us (97%)
  local copies, waits for them, and re-layouts  1.88 us (1%)
    pallas_call x1, Pallas kernels, shards(): pl.pallas_call(functools.partial(layers_kernel, side, [*inputs, 'out', *s...  130 us

profile of v7, /device:TPU:513, one launch (start us, length us, event | category | flops | bytes accessed | tf_op | source)
XLA Modules:
  0.0 132.0 jit_solution(7867198085003246745)
XLA Ops:
  0.0 130.1 %shard_map.136 = bf16[128,2048]{1,0:T(8,128)(2,1)} custom-call(bf16[128,1024]{1,0:T(8,128)(2,1)} %refs_0_.1, bf16[128,1024]{1,0:T(8,128)(2,1)} %refs_1_.1, bf16[128,1024]{1,0:T(8,128)(2,1)} %refs_2_.1, f32[8,257]{1,0:T(8,128)} %refs_3_.1, f32[8,257]{1,0:T(8,128)} %refs_4_.1, bf16[32,1024]{1,0:T(8,128)(2,1)} %bitcast.5, bf16[32,1024]{1,0:T(8,128)(2,1)} %bitcast.6, ...), custom_call_target="tpu_custom_call" | custom-call | tf_op jit(solution)/shard_map/pallas_call | solution.py:951
  130.1 1.9 %copy.16 = bf16[128,2048]{1,0:T(8,128)(2,1)} copy(bf16[128,2048]{1,0:T(8,128)(2,1)} %shard_map.136) | data formatting | bytes 1048576

commit v8 on v7

--- a/solution.py
+++ b/solution.py
@@ -767,13 +767,13 @@
     g2.yevent(3, 0, 4)
 
     def between2():
+        g2.yevent(3, 4, 4)
         @pl.when(y > 0)
         def _():
             for k in range(shift):
                 for copy in halo2(side - shift + k):
                     copy.wait_recv()
 
-        g2.yevent(3, 4, 4)
 
     take_back, back2 = attend_rows(
         side, x, y, qs2, ks2, vs2, r["band2"], r["outs2"], r["mixed2"], r["sb2"], r["rb2"],

time: 134 us -> 132 us (0.985); the launches traced: 132 us -> 132 us
  no operation moved by 1% of the time
where the time goes in v8:
time: 132 us
  Pallas kernels  130 us (98%)
  local copies, waits for them, and re-layouts  1.88 us (1%)
    pallas_call x1, Pallas kernels, shards(): pl.pallas_call(functools.partial(layers_kernel, side, [*inputs, 'out', *s...  130 us

profile of v8, /device:TPU:513, one launch (start us, length us, event | category | flops | bytes accessed | tf_op | source)
XLA Modules:
  0.0 132.0 jit_solution(14634620804304570462)
XLA Ops:
  0.0 130.1 %shard_map.136 = bf16[128,2048]{1,0:T(8,128)(2,1)} custom-call(bf16[128,1024]{1,0:T(8,128)(2,1)} %refs_0_.1, bf16[128,1024]{1,0:T(8,128)(2,1)} %refs_1_.1, bf16[128,1024]{1,0:T(8,128)(2,1)} %refs_2_.1, f32[8,257]{1,0:T(8,128)} %refs_3_.1, f32[8,257]{1,0:T(8,128)} %refs_4_.1, bf16[32,1024]{1,0:T(8,128)(2,1)} %bitcast.5, bf16[32,1024]{1,0:T(8,128)(2,1)} %bitcast.6, ...), custom_call_target="tpu_custom_call" | custom-call | tf_op jit(solution)/shard_map/pallas_call | solution.py:951
  130.1 1.9 %copy.16 = bf16[128,2048]{1,0:T(8,128)(2,1)} copy(bf16[128,2048]{1,0:T(8,128)(2,1)} %shard_map.136) | data formatting | bytes 1048576
